TPU v7x, 32 devices: a whole 2x2x4 slice. The times are simulated.
32 devices in a mesh: grp: 2 (over y), kv: 8 (over z, core), tp: 2 (over x).
Axes of the slice: x: 2, y: 2, z: 4, core: 2. Of those that a mesh axis runs over, the one named last changes fastest.
Arguments:
- tokens: bfloat16 [4096, 2048], P(('grp', 'kv')), parts along dimension 0, may hold values from -100 to 100
- query_weight: bfloat16 [2048, 512], P(None, 'tp'), may hold values from -0.125 to 0.125
- key_weight: bfloat16 [2048, 256], P(None, 'tp'), may hold values from -0.125 to 0.125
- value_weight: bfloat16 [2048, 256], P(None, 'tp'), may hold values from -0.125 to 0.125
- gate_weight: bfloat16 [2, 2048, 8], replicated, may hold values from -0.125 to 0.125
- squeeze_key: bfloat16 [2048, 64], replicated, may hold values from -0.125 to 0.125
- squeeze_value: bfloat16 [2048, 64], replicated, may hold values from -0.125 to 0.125
- out_weight: bfloat16 [512, 2048], P(None, 'tp'), may hold values from -1 to 1
- out_gain: bfloat16 [2048], replicated, may hold values from 0.099609375 to 1.8984375
- chosen: int32 [64, 32], P(('grp', 'kv')), parts along dimension 0, may hold values from -1 to 31, as said below
Outputs:
- output: bfloat16 [4096, 2048], P(('grp', 'kv'), 'tp'), parts along dimension 0
There are 2 independent parts, one for each index of `grp`. A program takes and returns all parts, laid end to end along the dimension named above; an argument that names none is the same for every part. Nothing has to cross between parts.
Inputs may be any that keep to these rules, and one draw needn't show every extreme that they name: `chosen`: row n lists distinct key blocks no later than n, always n itself, the rest -1. The query blocks of one device together choose at most 2 distinct blocks of any other device, and some device reaches that.
All inputs are finite; a program needn't handle non-finite values.
Results may differ from a plain program's by a relative error of at most 0.01.
The roundings to bfloat16 on the way count: a program that leaves them out, or rounds other values in their place, can miss the bound.
Values may be sent and summed in bfloat16 or wider, within the bound.
A program may use at most 64 MiB of HBM per device.

v0:
```python
import jax
import jax.numpy as jnp
from jax import lax
from jax.sharding import PartitionSpec as P

D = 2048
CMP_LEN = 32
SEL_BLOCK = 64
TOPN = 32


NEGATIVE = -1e30
EPSILON = 1e-06


def masked_weights(scores, allowed):
    masked = jnp.where(allowed, scores, NEGATIVE)
    row_peak = jnp.max(masked, axis=-1, keepdims=True)
    weights = jnp.where(allowed, jnp.exp(masked - row_peak), 0.0)
    weight_sum = jnp.sum(weights, axis=-1, keepdims=True)
    return (weights.astype(jnp.bfloat16), weight_sum)


def body(
    tokens,
    query_weight,
    key_weight,
    value_weight,
    gate_weight,
    squeeze_key,
    squeeze_value,
    out_weight,
    out_gain,
    chosen,
):
    tok_rows, model_width = tokens.shape
    head_size = squeeze_key.shape[1]
    kv_local = key_weight.shape[1] // head_size
    heads_local = query_weight.shape[1] // head_size
    group_size = heads_local // kv_local
    feature = 2 * kv_local * head_size
    blocks_local = tok_rows // SEL_BLOCK
    my_index = lax.axis_index("kv")
    head_index = lax.axis_index("tp")
    columns_local = out_weight.shape[1]
    offset = my_index * tok_rows
    score_scale = head_size ** (-0.5)
    gram_matrix = lax.psum(
        jnp.dot(out_weight, jnp.transpose(out_weight), preferred_element_type=jnp.float32).astype(
            jnp.bfloat16
        ),
        "tp",
    ).astype(jnp.float32)
    gram_high = lax.optimization_barrier(gram_matrix.astype(jnp.bfloat16))
    gram_low = (gram_matrix - gram_high.astype(jnp.float32)).astype(jnp.bfloat16)
    queries = jnp.dot(tokens, query_weight, preferred_element_type=jnp.float32).astype(jnp.bfloat16)
    both_weights = jnp.concatenate(
        [
            key_weight.reshape(model_width, kv_local, 1, head_size),
            value_weight.reshape(model_width, kv_local, 1, head_size),
        ],
        axis=2,
    ).reshape(model_width, feature)
    kv_pairs = jnp.dot(tokens, both_weights, preferred_element_type=jnp.float32).astype(
        jnp.bfloat16
    )
    gate_all = jax.nn.sigmoid(
        jnp.einsum("td,bdh->tbh", tokens, gate_weight, preferred_element_type=jnp.float32)
    )
    gate_values = lax.dynamic_slice_in_dim(gate_all, head_index * heads_local, heads_local, 2)
    squeeze_rows = tok_rows // CMP_LEN
    split_pairs = kv_pairs.reshape(squeeze_rows, CMP_LEN, kv_local, 2, head_size)
    key_flat = (
        split_pairs[:, :, :, 0]
        .transpose(0, 2, 1, 3)
        .reshape(squeeze_rows * kv_local, CMP_LEN * head_size)
    )
    value_flat = (
        split_pairs[:, :, :, 1]
        .transpose(0, 2, 1, 3)
        .reshape(squeeze_rows * kv_local, CMP_LEN * head_size)
    )
    small_keys = (
        jnp.dot(key_flat, squeeze_key, preferred_element_type=jnp.float32)
        .astype(jnp.bfloat16)
        .reshape(squeeze_rows, kv_local, 1, head_size)
    )
    small_values = (
        jnp.dot(value_flat, squeeze_value, preferred_element_type=jnp.float32)
        .astype(jnp.bfloat16)
        .reshape(squeeze_rows, kv_local, 1, head_size)
    )
    packed = jnp.concatenate([small_keys, small_values], axis=2).reshape(squeeze_rows, feature)
    summary = lax.all_gather(packed, "kv", axis=0, tiled=True).reshape(-1, kv_local, 2, head_size)
    summary_keys = summary[:, :, 0]
    summary_values = summary[:, :, 1]
    summary_end = jnp.arange(summary.shape[0], dtype=jnp.int32) * CMP_LEN + (CMP_LEN - 1)
    flat_ids = chosen.reshape(-1)
    everything = lax.all_gather(kv_pairs, "kv", axis=0, tiled=True).reshape(-1, SEL_BLOCK, feature)
    picked = jnp.take(everything, jnp.maximum(flat_ids, 0), axis=0)
    halves = 2
    half_blocks = blocks_local // halves
    half_rows = tok_rows // halves
    queries_split = queries.reshape(halves, half_rows, kv_local, group_size, head_size)
    picked_split = picked.reshape(halves, half_blocks, TOPN * SEL_BLOCK, kv_local, 2, head_size)
    chosen_split = chosen.reshape(halves, half_blocks, TOPN)
    starts = offset + jnp.arange(halves, dtype=jnp.int32) * half_rows

    def one_half(operands):
        part_queries, part_picked, part_chosen, first_row = operands
        positions = first_row + jnp.arange(half_rows, dtype=jnp.int32)
        scores = (
            jnp.einsum(
                "tkgd,ckd->tkgc", part_queries, summary_keys, preferred_element_type=jnp.float32
            )
            * score_scale
        )
        allowed = (summary_end[None, :] <= positions[:, None])[:, None, None, :]
        weights, weight_sum = masked_weights(scores, allowed)
        squeezed = jnp.einsum(
            "tkgc,ckd->tkgd", weights, summary_values, preferred_element_type=jnp.float32
        ) / jnp.maximum(weight_sum, 1.0)
        block_queries = part_queries.reshape(
            half_blocks, SEL_BLOCK, kv_local, group_size, head_size
        )
        scores = (
            jnp.einsum(
                "nqkgd,npkd->nqkgp",
                block_queries,
                part_picked[:, :, :, 0],
                preferred_element_type=jnp.float32,
            )
            * score_scale
        )
        key_positions = (
            jnp.maximum(part_chosen, 0)[:, :, None] * SEL_BLOCK
            + jnp.arange(SEL_BLOCK, dtype=jnp.int32)[None, None, :]
        ).reshape(half_blocks, TOPN * SEL_BLOCK)
        usable = jnp.repeat(part_chosen >= 0, SEL_BLOCK, axis=1)
        query_positions = positions.reshape(half_blocks, SEL_BLOCK)
        allowed = (usable[:, None, :] & (key_positions[:, None, :] <= query_positions[:, :, None]))[
            :, :, None, None, :
        ]
        weights, weight_sum = masked_weights(scores, allowed)
        selected = (
            jnp.einsum(
                "nqkgp,npkd->nqkgd",
                weights,
                part_picked[:, :, :, 1],
                preferred_element_type=jnp.float32,
            )
            / weight_sum
        )
        return (squeezed, selected.reshape(half_rows, kv_local, group_size, head_size))

    squeezed, selected = lax.map(one_half, (queries_split, picked_split, chosen_split, starts))
    squeezed = squeezed.reshape(tok_rows, heads_local, head_size)
    selected = selected.reshape(tok_rows, heads_local, head_size)
    mixed_heads = (
        (gate_values[:, 0, :, None] * squeezed + gate_values[:, 1, :, None] * selected)
        .reshape(tok_rows, heads_local * head_size)
        .astype(jnp.bfloat16)
    )
    whole_heads = lax.all_gather(mixed_heads, "tp", axis=1, tiled=True)
    projected = jnp.dot(whole_heads, out_weight, preferred_element_type=jnp.float32)
    through_gram = jnp.dot(whole_heads, gram_high, preferred_element_type=jnp.float32) + jnp.dot(
        whole_heads, gram_low, preferred_element_type=jnp.float32
    )
    squares = jnp.sum(through_gram * whole_heads.astype(jnp.float32), axis=1)
    gain_local = lax.dynamic_slice_in_dim(
        out_gain, head_index * columns_local, columns_local, 0
    ).astype(jnp.float32)
    normed = projected * lax.rsqrt(squares[:, None] / D + EPSILON) * gain_local[None, :]
    return normed.astype(jnp.bfloat16)


def solution(mesh):
    in_specs = (
        P(("grp", "kv"), None),
        P(None, "tp"),
        P(None, "tp"),
        P(None, "tp"),
        P(),
        P(),
        P(),
        P(None, "tp"),
        P(),
        P(("grp", "kv"), None),
    )
    out_specs = P(("grp", "kv"), "tp")
    return jax.shard_map(body, mesh=mesh, in_specs=in_specs, out_specs=out_specs, check_vma=False)
```

profile of v0, /device:TPU:0, one launch (start us, length us, event | category | flops | bytes accessed | tf_op | source)
XLA Modules:
  0.0 145.9 jit_solution(2844601919455153859)
XLA Ops:
  7.4 1.2 copy-done
  8.6 1.5 %convolution_convert_fusion = bf16[512,512]{1,0:T(8,128)(2,1)} fusion(bf16[512,1024]{1,0:T(8,128)(2,1)S(1)} %copy-done), kind=kOutput, calls=%fused_computation.57 | convolution fusion | flops 537133056 | bytes 1572864 | tf_op jit(solution)/shard_map/dot_general | solution.py:49
  10.4 1.3 copy.43
  12.0 1.1 fusion.48
  13.1 1.0 copy.45
  14.3 0.5 fusion.61
  15.0 1.1 convolution_convert_fusion.4
  16.4 1.1 convolution_convert_fusion.3
  17.7 15.9 %all_gather.9 = bf16[64,256]{1,0:T(8,128)(2,1)S(1)} all-gather(bf16[8,256]{1,0:T(8,128)(2,1)S(1)} %reshape.176), channel_id=1, replica_groups=mesh['grp'=2,'kv'=8,'tp'=2] {'kv'}, dimensions={0}, use_global_device_ids=true | all-gather | bytes 36864 | tf_op jit(solution)/shard_map/all_gather | solution.py:94
  33.8 0.7 copy.69
  34.8 1.1 convolution_convert_fusion.2
  35.9 1.1 reshape.198
  37.0 0.8 copy.54
  37.8 1.2 convolution_bitcast_fusion.1
  39.1 0.8 copy.58
  40.0 0.9 copy.61
  40.9 1.0 all-reduce.2.cloned.1.call-done
  41.9 1.5 %copy.52 = bf16[2048,256]{1,0:T(8,128)(2,1)S(1)} copy(bf16[2048,256]{0,1:T(8,128)(2,1)} %all-gather.2.cloned.1.call-done) | data formatting | bytes 2097152 | tf_op jit(solution)/shard_map/all_gather | solution.py:99
  43.4 2.8 %gather_fusion = bf16[128,64,256]{2,1,0:T(8,128)(2,1)} fusion(bf16[32,64,256]{2,1,0:T(8,128)(2,1)S(1)} %bitcast.183, s32[1024]{0:T(1024)S(1)} %pad_clamp_fusion), kind=kCustom, calls=%fused_computation | custom fusion | bytes 8389120 | tf_op jit(solution)/shard_map/jit(_take)/gather | solution.py:100
  46.1 15.1 %reshape.199 = bf16[2,2,2048,2,2,64]{5,4,3,2,1,0:T(2,128)(2,1)} reshape(bf16[128,64,256]{2,1,0:T(8,128)(2,1)} %gather_fusion) | data formatting | bytes 8388608 | tf_op jit(solution)/shard_map/jit(_take)/gather | solution.py:100
  61.2 21.2 %copy.70 = bf16[2,2,2048,2,2,64]{2,1,0,5,4,3:T(2,128)(2,1)} copy(bf16[2,2,2048,2,2,64]{5,4,3,2,1,0:T(2,128)(2,1)} %reshape.199) | data formatting | bytes 8388608 | tf_op jit(solution)/shard_map/jit(_take)/gather | solution.py:100
  82.4 7.8 %broadcast_select_fusion = bf16[2,2,2048,2,2,64]{2,1,0,5,4,3:T(2,128)(2,1)} fusion(bf16[2,2,2048,2,2,64]{2,1,0,5,4,3:T(2,128)(2,1)} %copy.70, pred[2,2,2048]{2,1,0:T(4,128)(4,1)S(1)} %broadcast_in_dim.75), kind=kLoop, calls=%fused_computation.53 | loop fusion | flops 2097152 | bytes 8396800 | tf_op jit(solution)/shard_map/jit(_take)/select_n | solution.py:100
  90.2 36.0 %while.13 = (s32[]{:T(128)}, f32[2,128,2,2,64]{1,4,3,2,0:T(8,128)}, f32[2,128,2,2,64]{1,4,3,2,0:T(8,128)}, s32[2]{0:T(128)S(1)}, bf16[2,128,2,2,64]{1,4,3,2,0:T(...) while((s32[]{:T(128)}, f32[2,128,2,2,64]{1,4,3,2,0:T(8,128)}, ...), condition=%wide.region_5.6_spmd.clone, body=%wide.region_0.5_spmd.clone.sunk | while | flops 288243648 | bytes 19728708 | solution.py:156
  90.7 0.6 dynamic_slice.53
  91.3 0.6 add_add_fusion.2
  92.2 0.9 constant_dynamic-slice_fusion.5
  93.0 0.8 reshape.203
  93.8 3.4 %constant_dynamic-slice_fusion.6 = bf16[1,2,2048,2,2,64]{2,1,0,5,4,3:T(2,128)(2,1)S(1)} fusion(bf16[2,2,2048,2,2,64]{2,1,0,5,4,3:T(2,128)(2,1)} %get-tuple-element.223, s32[]{:T(128)} %get-tuple-element.206), kind=kLoop, calls=%fused_computation.40.clone.1 | loop fusion | bytes 4194308 | tf_op jit(solution)/shard_map/while/body/jit(dynamic_index_in_dim)/dynamic_slice | solution.py:156
  97.2 0.9 copy.95
  98.1 4.2 %fusion.108 = (f32[2,64,2,2]{1,3,2,0:T(2,128)S(1)}, bf16[2,64,2,2,2048]{4,1,3,2,0:T(8,128)(2,1)}) fusion(pred[2,64,2048]{2,1,0:T(8,128)(4,1)S(1)} %compare_and_fusion.2, bf16[2,2048,2,2,64]{1,4,2,0,3:T(8,128)(2,1)S(1)} %bitcast.181, bf16[2,64,2,2,64]{1,0,4,3,2:T(2,128)(2,1)} %reshape.203), kind=kOutput, calls=%fused_computation.88.clone.1 | convolution fusion | flops 140511232 | bytes 3737600 | tf_op jit(solution)/shard_map/while/body/eval_jaxpr/sub | solution.py:19
  102.3 2.8 %fusion.109 = f32[2,64,2,2,64]{1,4,3,2,0:T(8,128)S(1)} fusion(bf16[2,64,2,2,2048]{4,1,3,2,0:T(8,128)(2,1)} %get-tuple-element.194, bf16[2,2048,2,2,64]{1,4,2,0,3:T(8,128)(2,1)S(1)} %bitcast.182, f32[2,64,2,2]{1,3,2,0:T(2,128)S(1)} %get-tuple-element.195), kind=kOutput, calls=%fused_computation.14.clone.1 | convolution fusion | flops 134250496 | bytes 3280896 | tf_op jit(solution)/shard_map/while/body/eval_jaxpr/nqkgp,npkd->nqkgd/dot_general | solution.py:146
  105.5 0.6 iota_add_fusion.2
  106.6 1.6 %fusion.107 = f32[2,128,2,2,64]{1,4,3,2,0:T(8,128)} fusion(f32[2,128,2,2,64]{1,4,3,2,0:T(8,128)} %get-tuple-element.207, s32[]{:T(128)} %get-tuple-element.206, f32[128,2,2]{0,2,1:T(2,128)S(1)} %broadcast_maximum_fusion.3, bf16[64,2,64]{0,2,1:T(8,128)(2,1)} %get-tuple-element.222, f32[128,2,2,64]{0,3,2,1:T(8,128)S(1)} %fusion.106, ...), kind=kOutput, calls=%fused_computation.21.clone.1 | convolution fusion | flops 4325951 | bytes 436736 | tf_op jit(solution)/shard_map/while/body/eval_jaxpr/tkgc,ckd->tkgd/dot_general | solution.py:120
  108.7 0.6 dynamic_slice.53
  109.3 0.6 add_add_fusion.2
  110.1 0.9 constant_dynamic-slice_fusion.5
  111.0 0.8 reshape.203
  111.8 3.4 %constant_dynamic-slice_fusion.6 = bf16[1,2,2048,2,2,64]{2,1,0,5,4,3:T(2,128)(2,1)S(1)} fusion(bf16[2,2,2048,2,2,64]{2,1,0,5,4,3:T(2,128)(2,1)} %get-tuple-element.223, s32[]{:T(128)} %get-tuple-element.206), kind=kLoop, calls=%fused_computation.40.clone.1 | loop fusion | bytes 4194308 | tf_op jit(solution)/shard_map/while/body/jit(dynamic_index_in_dim)/dynamic_slice | solution.py:156
  115.2 0.9 copy.95
  116.1 4.2 %fusion.108 = (f32[2,64,2,2]{1,3,2,0:T(2,128)S(1)}, bf16[2,64,2,2,2048]{4,1,3,2,0:T(8,128)(2,1)}) fusion(pred[2,64,2048]{2,1,0:T(8,128)(4,1)S(1)} %compare_and_fusion.2, bf16[2,2048,2,2,64]{1,4,2,0,3:T(8,128)(2,1)S(1)} %bitcast.181, bf16[2,64,2,2,64]{1,0,4,3,2:T(2,128)(2,1)} %reshape.203), kind=kOutput, calls=%fused_computation.88.clone.1 | convolution fusion | flops 140511232 | bytes 3737600 | tf_op jit(solution)/shard_map/while/body/eval_jaxpr/sub | solution.py:19
  120.3 2.8 %fusion.109 = f32[2,64,2,2,64]{1,4,3,2,0:T(8,128)S(1)} fusion(bf16[2,64,2,2,2048]{4,1,3,2,0:T(8,128)(2,1)} %get-tuple-element.194, bf16[2,2048,2,2,64]{1,4,2,0,3:T(8,128)(2,1)S(1)} %bitcast.182, f32[2,64,2,2]{1,3,2,0:T(2,128)S(1)} %get-tuple-element.195), kind=kOutput, calls=%fused_computation.14.clone.1 | convolution fusion | flops 134250496 | bytes 3280896 | tf_op jit(solution)/shard_map/while/body/eval_jaxpr/nqkgp,npkd->nqkgd/dot_general | solution.py:146
  123.5 0.6 iota_add_fusion.2
  124.6 1.6 %fusion.107 = f32[2,128,2,2,64]{1,4,3,2,0:T(8,128)} fusion(f32[2,128,2,2,64]{1,4,3,2,0:T(8,128)} %get-tuple-element.207, s32[]{:T(128)} %get-tuple-element.206, f32[128,2,2]{0,2,1:T(2,128)S(1)} %broadcast_maximum_fusion.3, bf16[64,2,64]{0,2,1:T(8,128)(2,1)} %get-tuple-element.222, f32[128,2,2,64]{0,3,2,1:T(8,128)S(1)} %fusion.106, ...), kind=kOutput, calls=%fused_computation.21.clone.1 | convolution fusion | flops 4325951 | bytes 436736 | tf_op jit(solution)/shard_map/while/body/eval_jaxpr/tkgc,ckd->tkgd/dot_general | solution.py:120
  126.2 1.3 copy.71
  128.0 1.3 copy.72
  129.7 1.1 add_convert_fusion
  130.8 5.7 %all_gather.11 = bf16[256,512]{1,0:T(8,128)(2,1)S(1)} all-gather(bf16[256,256]{1,0:T(8,128)(2,1)S(1)} %add_convert_fusion), channel_id=1, replica_groups=mesh['grp'=2,'kv'=8,'tp'=2] {'tp'}, dimensions={1}, use_global_device_ids=true | all-gather | bytes 393216 | tf_op jit(solution)/shard_map/all_gather | solution.py:164
  137.3 1.2 fusion.45
  (95 shorter events, 6.6 us)
Async XLA Ops:
  7.4 1.2 copy-start
  7.4 2.8 %copy-start.3 = (bf16[2048,128]{1,0:T(8,128)(2,1)S(1)}, bf16[2048,128]{1,0:T(8,128)(2,1)}, u32[]{:S(2)}) copy-start(bf16[2048,128]{1,0:T(8,128)(2,1)} %param.14) | copy-start | bytes 1572868
  7.4 34.5 %all-reduce.2.cloned.1.call-start = ((), (), s32[]{:S(2)}) async-start(), calls=%async_computation.1 | async-start | bytes 1048576 | tf_op jit(solution)/shard_map/psum | solution.py:48
  10.1 1.8 %copy-start.1 = (bf16[256,2048]{1,0:T(8,128)(2,1)S(1)}, bf16[256,2048]{1,0:T(8,128)(2,1)}, u32[]{:S(2)}) copy-start(bf16[256,2048]{1,0:T(8,128)(2,1)} %param.12) | copy-start | bytes 3145732
  10.2 31.7 %all-gather.2.cloned.1.call-start = ((), (), s32[]{:S(2)}) async-start(), calls=%async_computation | async-start | bytes 1179648 | tf_op jit(solution)/shard_map/all_gather | solution.py:99
  11.8 22.7 %copy-start.7 = (s32[4,32]{1,0:T(4,128)S(1)}, s32[4,32]{1,0:T(4,128)}, u32[]{:S(2)}) copy-start(s32[4,32]{1,0:T(4,128)} %param.21) | copy-start | bytes 1540
  11.8 23.0 %copy-start.2 = (bf16[2048,256]{1,0:T(8,128)(2,1)S(1)}, bf16[2048,256]{1,0:T(8,128)(2,1)}, u32[]{:S(2)}) copy-start(bf16[2048,256]{1,0:T(8,128)(2,1)} %param.13) | copy-start | bytes 3145732
  14.8 26.0 %copy-start.8 = (bf16[2048]{0:T(1024)(128)(2,1)S(1)}, bf16[2048]{0:T(1024)(128)(2,1)}, u32[]{:S(2)}) copy-start(bf16[2048]{0:T(1024)(128)(2,1)} %param.20) | copy-start | bytes 12292
  102.3 3.2 %copy-start.5 = (f32[2,128,2,2,64]{1,4,3,2,0:T(8,128)S(1)}, f32[2,128,2,2,64]{1,4,3,2,0:T(8,128)}, u32[]{:S(2)}) copy-start(f32[2,128,2,2,64]{1,4,3,2,0:T(8,128)} %get-tuple-element.208) | copy-start | bytes 786436 | tf_op jit(solution)/shard_map/while
  105.5 0.7 copy-start.6
  120.3 3.2 %copy-start.5 = (f32[2,128,2,2,64]{1,4,3,2,0:T(8,128)S(1)}, f32[2,128,2,2,64]{1,4,3,2,0:T(8,128)}, u32[]{:S(2)}) copy-start(f32[2,128,2,2,64]{1,4,3,2,0:T(8,128)} %get-tuple-element.208) | copy-start | bytes 786436 | tf_op jit(solution)/shard_map/while
  123.4 0.7 copy-start.6
  126.2 10.4 %copy-start.4 = (bf16[512,512]{1,0:T(8,128)(2,1)S(1)}, bf16[512,512]{1,0:T(8,128)(2,1)}, u32[]{:S(2)}) copy-start(bf16[512,512]{1,0:T(8,128)(2,1)} %all-reduce.2.cloned.1.call-done) | copy-start | bytes 1572868
Sparse Core Ops, SparseCore 0:
  10.5 31.3 all-reduce.1
Sparse Core Ops, SparseCore 1:
  13.2 26.7 all-gather.1
where the time goes:
time: 148 us; the launch traced here: 146 us
  local copies, waits for them, and re-layouts  68.7 us (46%)
  matrix products  26.9 us (18%)
  blocking collectives  21.6 us (15%)
  between operations  15.1 us (10%)
  other arithmetic  12.2 us (8%)
    gather x3, local copies, waits for them, and re-layouts, body(): picked = jnp.take(everything, jnp.maximum(flat_ids, 0), axis=0)  39.1 us
    all_gather x1, blocking collectives, body(): lax.all_gather(packed, 'kv', axis=0, tiled=True)  15.9 us
    dynamic_slice x8, local copies, waits for them, and re-layouts, body(): lax.map(one_half, (queries_split, picked_split, chosen_split, starts))  11.6 us
    sub x4, matrix products, masked_weights(): weights = jnp.where(allowed, jnp.exp(masked - row_peak), 0.0)  8.74 us
    select_n x1, other arithmetic, body(): picked = jnp.take(everything, jnp.maximum(flat_ids, 0), axis=0)  7.77 us
    all_gather x1, blocking collectives, body(): whole_heads = lax.all_gather(mixed_heads, 'tp', axis=1, tiled=True)  5.73 us
    dot_general x2, matrix products, one_half(): jnp.einsum('nqkgp,npkd->nqkgd', weights, part_picked[:, :, :, 1], preferr...  5.51 us
    unnamed x17, local copies, waits for them, and re-layouts  3.53 us
  transfers between devices with their start and end apart: 2, of which 1 were waited for; matrix products, arithmetic and copies ran while one was open for 10% of the time, Pallas kernels for 0%

commit v1 on v0

v1 whole, which is shorter than its diff:
```python
import functools

import jax
import jax.numpy as jnp
from jax import lax
from jax.experimental import pallas as pl
from jax.experimental.pallas import tpu as pltpu
from jax.sharding import PartitionSpec as P

CMP_LEN = 32
SEL_BLOCK = 64
NEGATIVE = -1e30
EPSILON = 1e-06
MESH = pl.DeviceIdType.MESH
NT = (((1,), (1,)), ((), ()))


def kernel(
    n,
    dims,
    chosen_ref,
    tok_hbm,
    qw_hbm,
    kw_hbm,
    vw_hbm,
    gw_hbm,
    sqk_hbm,
    sqv_hbm,
    ow_hbm,
    out_ref,
    tok,
    weights,
    kw,
    vw,
    gw,
    sqk,
    sqv,
    ow,
    kv,
    kvf,
    summ,
    bias,
    q,
    gates,
    m_ref,
    l_ref,
    acc_ref,
    mix,
    sq,
    load_sem,
    recv_sem,
    up_sem,
    across_sem,
    tp_send,
    tp_recv,
):
    rows, width, hs, kvl, group, total_cols, tps = dims
    chips = n // 2
    nq = rows // SEL_BLOCK
    qcols = kvl * group * hs
    feat = 2 * hs
    cmp_rows = rows // CMP_LEN
    unit = group * SEL_BLOCK
    me = lax.axis_index("kv")
    tp = lax.axis_index("tp")
    z = me // 2
    core = me - 2 * z
    mate = 2 * z + 1 - core
    has_up = z < chips - 1
    parts = kvl + 1

    kcols = kvl * hs
    joint = kcols % 128 == 0
    if joint:
        kw = weights.at[:, pl.ds(qcols, kcols)]
        vw = weights.at[:, pl.ds(qcols + kcols, kcols)]
    loads = [
        pltpu.make_async_copy(tok_hbm, tok, load_sem.at[0]),
        pltpu.make_async_copy(kw_hbm, kw, load_sem.at[1]),
        pltpu.make_async_copy(vw_hbm, vw, load_sem.at[2]),
        pltpu.make_async_copy(sqk_hbm, sqk, load_sem.at[3]),
        pltpu.make_async_copy(sqv_hbm, sqv, load_sem.at[4]),
        pltpu.make_async_copy(qw_hbm, weights.at[:, pl.ds(0, qcols)], load_sem.at[5]),
        pltpu.make_async_copy(gw_hbm, gw, load_sem.at[6]),
        pltpu.make_async_copy(ow_hbm, ow, load_sem.at[7]),
    ]
    for load in loads:
        load.start()

    barrier = pltpu.get_barrier_semaphore()
    pl.semaphore_signal(barrier, inc=1, device_id={"kv": mate}, device_id_type=MESH)
    for d in range(1, tps):
        pl.semaphore_signal(
            barrier, inc=1, device_id={"tp": lax.rem(tp + d, tps)}, device_id_type=MESH
        )

    @pl.when(z > 0)
    def _():
        pl.semaphore_signal(barrier, inc=1, device_id={"kv": me - 2}, device_id_type=MESH)

    ids = chosen_ref[...]
    lane_row = lax.broadcasted_iota(jnp.int32, (nq, rows), 1)

    def make_bias(j, carry):
        row = jnp.zeros((nq, rows), jnp.float32)
        for b in range(nq):
            hit = jnp.max(jnp.where(ids == j * nq + b, 1.0, 0.0), axis=1, keepdims=True)
            here = (lane_row >= b * SEL_BLOCK) & (lane_row < (b + 1) * SEL_BLOCK)
            row = jnp.where(here, hit, row)
        bias[j, 0:nq, :] = jnp.where(row > 0.5, 0.0, NEGATIVE)
        return carry

    lax.fori_loop(0, me + 1, make_bias, 0)

    def clear(j, carry):
        summ[j] = jnp.zeros((cmp_rows, kvl * feat), jnp.float32)
        return carry

    lax.fori_loop(me + 1, n, clear, 0)

    for i in range(3):
        loads[i].wait()
    if joint:
        pairs = jnp.dot(
            tok[...], weights[:, qcols : qcols + 2 * kcols], preferred_element_type=jnp.float32
        )
        sides = [pairs[:, :kcols], pairs[:, kcols:]]
    else:
        sides = [
            jnp.dot(tok[...], w[...], preferred_element_type=jnp.float32) for w in (kw, vw)
        ]
    sides = [side.astype(jnp.bfloat16).astype(jnp.float32) for side in sides]
    for i, side in enumerate(sides):
        if not joint:
            side = jnp.concatenate([side, jnp.zeros((rows, 128 - kcols), jnp.float32)], axis=1)
        kvf[i] = side
    for k in range(kvl):
        kv[me, k] = jnp.concatenate(
            [side[:, k * hs : (k + 1) * hs] for side in sides], axis=1
        ).astype(jnp.bfloat16)

    def piece(source, part):
        return summ.at[source] if part == kvl else kv.at[source, part]

    def upward(source, part):
        return pltpu.make_async_remote_copy(
            src_ref=piece(source, part),
            dst_ref=piece(source, part),
            send_sem=up_sem.at[source // 2, part],
            recv_sem=recv_sem.at[source, part],
            device_id={"kv": me + 2},
            device_id_type=MESH,
        )

    def across(source, part):
        return pltpu.make_async_remote_copy(
            src_ref=piece(source, part),
            dst_ref=piece(source, part),
            send_sem=across_sem.at[source // 2, part],
            recv_sem=recv_sem.at[source, part],
            device_id={"kv": mate},
            device_id_type=MESH,
        )

    pl.semaphore_wait(barrier, tps + jnp.minimum(chips - 1 - z, 1))

    def send_own(part):
        @pl.when(has_up)
        def _():
            upward(me, part).start()

        @pl.when(core == 0)
        def _():
            across(me, part).start()

    for k in range(kvl):
        send_own(k)

    loads[3].wait()
    loads[4].wait()
    squeezed = []
    for side, weight in ((0, sqk), (1, sqv)):
        tiles = []
        for p in range(0, CMP_LEN, 2):
            a = kvf[side, pl.ds(p, cmp_rows, stride=CMP_LEN), :]
            b = kvf[side, pl.ds(p + 1, cmp_rows, stride=CMP_LEN), :]
            heads = [
                jnp.concatenate([x[:, k * hs : (k + 1) * hs] for x in (a, b)], axis=1)
                for k in range(kvl)
            ]
            tiles.append(jnp.concatenate(heads, axis=0))
        flat = jnp.concatenate(tiles, axis=1).astype(jnp.bfloat16)
        squeezed.append(
            lax.dot_general(flat, weight[...], NT, preferred_element_type=jnp.float32)
            .astype(jnp.bfloat16)
            .astype(jnp.float32)
        )
    summ[me] = jnp.concatenate(
        [
            half[k * cmp_rows : (k + 1) * cmp_rows]
            for k in range(kvl)
            for half in squeezed
        ],
        axis=1,
    )
    send_own(kvl)

    loads[5].wait()
    scale = hs ** (-0.5)
    queries = (
        jnp.dot(tok[...], weights[:, :qcols], preferred_element_type=jnp.float32)
        .astype(jnp.bfloat16)
        .astype(jnp.float32)
        * scale
    )
    low_q = lax.broadcasted_iota(jnp.int32, (SEL_BLOCK, feat), 1) < hs
    for k in range(kvl):
        for b in range(nq):
            tile = queries[b * SEL_BLOCK : (b + 1) * SEL_BLOCK, k * feat : (k + 1) * feat]
            q[k, b * unit : b * unit + SEL_BLOCK, :] = jnp.where(low_q, tile, 0.0).astype(
                jnp.bfloat16
            )
            q[k, b * unit + SEL_BLOCK : (b + 1) * unit, :] = jnp.where(
                low_q, pltpu.roll(tile, hs, 1), 0.0
            ).astype(jnp.bfloat16)
    loads[6].wait()
    hl = kvl * group
    every = jax.nn.sigmoid(
        lax.dot_general(tok[...], gw[...], NT, preferred_element_type=jnp.float32)
    )
    for branch in range(2):
        base = branch * tps * hl
        mine = every[:, base : base + hl]
        for t in range(1, tps):
            mine = jnp.where(tp == t, every[:, base + t * hl : base + (t + 1) * hl], mine)
        gates[branch] = mine

    def attend(source, k, first):
        keys = kv[source, k]
        for b in range(nq):
            at = pl.ds(b * unit, unit)
            s = lax.dot_general(q[k, at, :], keys, NT, preferred_element_type=jnp.float32)
            s = s + bias[source, b : b + 1, :]
            if first:
                col = lax.broadcasted_iota(jnp.int32, (SEL_BLOCK, rows), 1)
                row = lax.broadcasted_iota(jnp.int32, (SEL_BLOCK, rows), 0)
                seen = col <= row + b * SEL_BLOCK
                s = jnp.concatenate(
                    [
                        jnp.where(seen, s[:SEL_BLOCK], NEGATIVE),
                        jnp.where(seen, s[SEL_BLOCK:], NEGATIVE),
                    ],
                    axis=0,
                )
            peak = jnp.broadcast_to(jnp.max(s, axis=1, keepdims=True), (unit, feat))
            if not first:
                before = m_ref[k, at, :]
                peak = jnp.maximum(before, peak)
                alpha = jnp.exp(before - peak)
            p = jnp.exp(s - jnp.concatenate([peak] * (rows // feat), axis=1))
            sums = p[:, :feat]
            for i in range(1, rows // feat):
                sums = sums + p[:, i * feat : (i + 1) * feat]
            got = jnp.dot(p.astype(jnp.bfloat16), keys, preferred_element_type=jnp.float32)
            if not first:
                sums = sums + l_ref[k, at, :] * alpha
                got = got + acc_ref[k, at, :] * alpha
            m_ref[k, at, :] = peak
            l_ref[k, at, :] = sums
            acc_ref[k, at, :] = got

    for k in range(kvl):
        attend(me, k, True)

    @pl.when(core == 1)
    def _():
        for k in range(kvl):
            across(me - 1, k).wait_recv()
            attend(me - 1, k, False)
        across(me - 1, kvl).wait_recv()

    def step(s, carry):
        mine = me - 2 * s
        other = mate - 2 * s

        def take(part):
            upward(mine, part).wait_recv()

            @pl.when(has_up)
            def _():
                upward(mine, part).start()

            across(mine, part).start()

        for k in range(kvl):
            take(k)
            attend(mine, k, False)
            across(other, k).wait_recv()
            attend(other, k, False)
        take(kvl)
        across(other, kvl).wait_recv()
        return carry

    lax.fori_loop(1, z + 1, step, 0)

    cols = n * cmp_rows
    for k in range(kvl):
        small = (
            summ[:, :, k * feat : (k + 1) * feat].reshape(cols, feat).astype(jnp.bfloat16)
        )
        for b in range(nq):
            at = pl.ds(b * unit, unit)
            s = lax.dot_general(q[k, at, :], small, NT, preferred_element_type=jnp.float32)
            col = lax.broadcasted_iota(jnp.int32, (SEL_BLOCK, cols), 1)
            row = lax.broadcasted_iota(jnp.int32, (SEL_BLOCK, cols), 0)
            seen = col * CMP_LEN + (CMP_LEN - 1) <= row + (me * rows + b * SEL_BLOCK)
            s0 = jnp.where(seen, s[:SEL_BLOCK], NEGATIVE)
            s1 = jnp.where(seen, s[SEL_BLOCK:], NEGATIVE)
            halves = []
            for half in (s0, s1):
                peak = jnp.max(half, axis=1, keepdims=True)
                halves.append(jnp.where(seen, jnp.exp(half - peak), 0.0))
            w = jnp.concatenate(halves, axis=0)
            low_sum = jnp.sum(w, axis=1, keepdims=True)
            comp = jnp.dot(w.astype(jnp.bfloat16), small, preferred_element_type=jnp.float32)
            comp = comp / jnp.maximum(low_sum, 1.0)
            sel = acc_ref[k, at, :] / jnp.sum(l_ref[k, at, :], axis=1, keepdims=True)
            pos = pl.ds(b * SEL_BLOCK, SEL_BLOCK)
            heads = []
            for g in range(group):
                h = k * group + g
                cut = slice(g * SEL_BLOCK, (g + 1) * SEL_BLOCK)
                heads.append(
                    gates[0, pos, h : h + 1] * comp[cut] + gates[1, pos, h : h + 1] * sel[cut]
                )
            mix[tp, pos, k * feat : (k + 1) * feat] = jnp.where(
                low_q, pltpu.roll(heads[0], hs, 1), heads[1]
            ).astype(jnp.bfloat16)

    def swap(ref, d, source, kind):
        return pltpu.make_async_remote_copy(
            src_ref=ref.at[source],
            dst_ref=ref.at[source],
            send_sem=tp_send.at[kind, d],
            recv_sem=tp_recv.at[kind, source],
            device_id={"tp": lax.rem(tp + d, tps)},
            device_id_type=MESH,
        )

    for d in range(1, tps):
        swap(mix, d, tp, 0).start()
    loads[7].wait()
    for d in range(1, tps):
        swap(mix, d, lax.rem(tp + d, tps), 0).wait_recv()
    proj = jnp.dot(mix[0], ow[:qcols, :], preferred_element_type=jnp.float32)
    for t in range(1, tps):
        proj = proj + jnp.dot(
            mix[t], ow[t * qcols : (t + 1) * qcols, :], preferred_element_type=jnp.float32
        )
    out_ref[...] = proj
    lanes = proj[:, :128] * proj[:, :128]
    for i in range(1, proj.shape[1] // 128):
        tile = proj[:, i * 128 : (i + 1) * 128]
        lanes = lanes + tile * tile
    sq[tp] = jnp.sum(lanes.T.reshape(16, 8, rows), axis=0)
    for d in range(1, tps):
        swap(sq, d, tp, 1).start()

    for part in range(parts):
        @pl.when(has_up)
        def _():
            upward(me, part).wait_send()

        @pl.when(core == 0)
        def _():
            across(me, part).wait_send()

    def drain(s, carry):
        mine = me - 2 * s
        for part in range(parts):
            @pl.when(has_up)
            def _():
                upward(mine, part).wait_send()

            across(mine, part).wait_send()
        return carry

    lax.fori_loop(1, z + 1, drain, 0)
    for d in range(1, tps):
        swap(sq, d, lax.rem(tp + d, tps), 1).wait_recv()
    squares = jnp.sum(jnp.sum(sq[...], axis=0), axis=0, keepdims=True)
    factor = lax.rsqrt(squares / total_cols + EPSILON)
    column = jnp.broadcast_to(factor, (128, rows)).T
    for i in range(out_ref.shape[1] // 128):
        out_ref[:, i * 128 : (i + 1) * 128] = out_ref[:, i * 128 : (i + 1) * 128] * column
    for d in range(1, tps):
        swap(mix, d, tp, 0).wait_send()
        swap(sq, d, tp, 1).wait_send()


def body(
    n,
    tps,
    tokens,
    query_weight,
    key_weight,
    value_weight,
    gate_weight,
    squeeze_key,
    squeeze_value,
    out_weight,
    out_gain,
    chosen,
):
    rows, width = tokens.shape
    hs = squeeze_key.shape[1]
    kvl = key_weight.shape[1] // hs
    qcols = query_weight.shape[1]
    group = qcols // hs // kvl
    cols = out_weight.shape[1]
    total_cols = out_gain.shape[0]
    feat = 2 * hs
    nq = rows // SEL_BLOCK
    stack = nq * group * SEL_BLOCK
    cmp_rows = rows // CMP_LEN
    dims = (rows, width, hs, kvl, group, total_cols, tps)
    kcols = kvl * hs
    joint = kcols % 128 == 0
    spare = (8, 128) if joint else (width, kcols)
    any_spec = pl.BlockSpec(memory_space=pl.ANY)
    vmem = pl.BlockSpec(memory_space=pltpu.VMEM)
    bf, f32 = jnp.bfloat16, jnp.float32
    dma = pltpu.SemaphoreType.DMA
    scaled = pl.pallas_call(
        functools.partial(kernel, n, dims),
        out_shape=jax.ShapeDtypeStruct((rows, cols), f32),
        in_specs=[vmem] + [any_spec] * 8,
        out_specs=vmem,
        scratch_shapes=[
            pltpu.VMEM((rows, width), bf),
            pltpu.VMEM((width, qcols + 2 * kcols if joint else qcols), bf),
            pltpu.VMEM(spare, bf),
            pltpu.VMEM(spare, bf),
            pltpu.VMEM((gate_weight.shape[0] * gate_weight.shape[2], width), bf),
            pltpu.VMEM(squeeze_key.shape[::-1], bf),
            pltpu.VMEM(squeeze_value.shape[::-1], bf),
            pltpu.VMEM(out_weight.shape, bf),
            pltpu.VMEM((n, kvl, rows, feat), bf),
            pltpu.VMEM((2, rows, max(kcols, 128)), f32),
            pltpu.VMEM((n, cmp_rows, kvl * feat), f32),
            pltpu.VMEM((n, 8, rows), f32),
            pltpu.VMEM((kvl, stack, feat), bf),
            pltpu.VMEM((2, rows, kvl * group), f32),
            pltpu.VMEM((kvl, stack, feat), f32),
            pltpu.VMEM((kvl, stack, feat), f32),
            pltpu.VMEM((kvl, stack, feat), f32),
            pltpu.VMEM((tps, rows, qcols), bf),
            pltpu.VMEM((tps, 8, rows), f32),
            dma((8,)),
            dma((n, kvl + 1)),
            dma((n // 2, kvl + 1)),
            dma((n // 2, kvl + 1)),
            dma((2, tps)),
            dma((2, tps)),
        ],
        compiler_params=pltpu.CompilerParams(
            collective_id=0, has_side_effects=True, vmem_limit_bytes=56 * 1024 * 1024
        ),
    )(
        chosen,
        tokens,
        query_weight,
        key_weight,
        value_weight,
        gate_weight.transpose(0, 2, 1).reshape(-1, width),
        squeeze_key.T,
        squeeze_value.T,
        out_weight,
    )
    gain = lax.dynamic_slice_in_dim(out_gain, lax.axis_index("tp") * cols, cols, 0)
    return (scaled * gain.astype(f32)[None, :]).astype(bf)


def solution(mesh):
    in_specs = (
        P(("grp", "kv"), None),
        P(None, "tp"),
        P(None, "tp"),
        P(None, "tp"),
        P(),
        P(),
        P(),
        P(None, "tp"),
        P(),
        P(("grp", "kv"), None),
    )
    return jax.shard_map(
        functools.partial(body, mesh.shape["kv"], mesh.shape["tp"]),
        mesh=mesh,
        in_specs=in_specs,
        out_specs=P(("grp", "kv"), "tp"),
        check_vma=False,
    )
```

time: 148 us -> 32.6 us (0.22)
  the two profiles are of different devices: /device:TPU:0 before, /device:TPU:30 now
where the time goes in v1:
time: 32.6 us; the launch traced here: 32.4 us
  Pallas kernels  29.6 us (91%)
  other arithmetic  2.12 us (7%)
  local copies, waits for them, and re-layouts  0.69 us (2%)
    pallas_call x1, Pallas kernels, body(): pl.pallas_call(functools.partial(kernel, n, dims), out_shape=jax.ShapeDty...  29.6 us
    convert_element_type x2, other arithmetic, body(): return (scaled * gain.astype(f32)[None, :]).astype(bf)  2.12 us
    unnamed x2, local copies, waits for them, and re-layouts  0.69 us

profile of v1, /device:TPU:30, one launch (start us, length us, event | category | flops | bytes accessed | tf_op | source)
XLA Modules:
  0.0 32.4 jit_solution(274142052800768626)
XLA Ops:
  0.0 0.0 copy-start
  0.0 0.7 %copy-done = bf16[2048]{0:T(1024)(128)(2,1)S(1)} copy-done((bf16[2048]{0:T(1024)(128)(2,1)S(1)}, bf16[2048]{0:T(1024)(128)(2,1)}, u32[]{:S(2)}) %copy-start) | copy-done | bytes 4120
  0.7 29.6 %shard_map.100 = f32[256,1024]{1,0:T(8,128)} custom-call(s32[4,32]{1,0:T(4,128)} %chosen_ref.1, bf16[256,2048]{1,0:T(8,128)(2,1)} %tok_hbm.1, bf16[2048,256]{1,0:T(8,128)(2,1)} %qw_hbm.1, bf16[2048,128]{1,0:T(8,128)(2,1)} %kw_hbm.1, bf16[2048,128]{1,0:T(8,128)(2,1)} %vw_hbm.1, bf16[16,2048]{1,0:T(8,128)(2,1)} %bitcast.7, bf16[64,2048]{1,0:T(8,128)(2,1)} %bitcast.5, ...), custom_call_target="tpu_custom_call" | custom-call | tf_op jit(solution)/shard_map/pallas_call | solution.py:434
  30.3 2.1 %multiply_convert_fusion = bf16[256,1024]{1,0:T(8,128)(2,1)} fusion(f32[256,1024]{1,0:T(8,128)} %shard_map.100, f32[1024]{0:T(1024)S(1)} %dynamic-slice_convert_fusion), kind=kLoop, calls=%fused_computation | loop fusion | flops 524288 | bytes 1576960 | tf_op jit(solution)/shard_map/convert_element_type | solution.py:481
  (1 shorter events, 0.0 us)
Async XLA Ops:
  0.0 0.7 %copy-start = (bf16[2048]{0:T(1024)(128)(2,1)S(1)}, bf16[2048]{0:T(1024)(128)(2,1)}, u32[]{:S(2)}) copy-start(bf16[2048]{0:T(1024)(128)(2,1)} %param.18) | copy-start | bytes 12292

commit v2 on v1

v2 whole, which is shorter than its diff:
```python
import functools

import jax
import jax.numpy as jnp
from jax import lax
from jax.experimental import pallas as pl
from jax.experimental.pallas import tpu as pltpu
from jax.sharding import PartitionSpec as P

CMP_LEN = 32
SEL_BLOCK = 64
NEGATIVE = -1e30
EPSILON = 1e-06
MESH = pl.DeviceIdType.MESH
NT = (((1,), (1,)), ((), ()))


def kernel(
    n,
    dims,
    chosen_ref,
    gain_ref,
    tok_hbm,
    qw_hbm,
    kw_hbm,
    vw_hbm,
    gw_hbm,
    sqk_hbm,
    sqv_hbm,
    ow_hbm,
    out_ref,
    tok,
    weights,
    kw,
    vw,
    gw,
    sqk,
    sqv,
    ow,
    keys,
    vals,
    kvf,
    summ,
    bias,
    q,
    gates,
    m_ref,
    l_ref,
    acc_ref,
    s_ref,
    p_ref,
    mix,
    sq,
    load_sem,
    recv_sem,
    up_sem,
    across_sem,
    tp_send,
    tp_recv,
):
    rows, width, hs, kvl, group, total_cols, tps = dims
    chips = n // 2
    nq = rows // SEL_BLOCK
    qcols = kvl * group * hs
    cmp_rows = rows // CMP_LEN
    lanes_q = group * rows
    me = lax.axis_index("kv")
    tp = lax.axis_index("tp")
    z = me // 2
    core = me - 2 * z
    mate = 2 * z + 1 - core
    has_up = z < chips - 1
    parts = 3

    kcols = kvl * hs
    joint = kcols % 128 == 0
    if joint:
        kw = weights.at[:, pl.ds(qcols, kcols)]
        vw = weights.at[:, pl.ds(qcols + kcols, kcols)]
    loads = [
        pltpu.make_async_copy(tok_hbm, tok, load_sem.at[0]),
        pltpu.make_async_copy(kw_hbm, kw, load_sem.at[1]),
        pltpu.make_async_copy(vw_hbm, vw, load_sem.at[2]),
        pltpu.make_async_copy(sqk_hbm, sqk, load_sem.at[3]),
        pltpu.make_async_copy(sqv_hbm, sqv, load_sem.at[4]),
        pltpu.make_async_copy(qw_hbm, weights.at[:, pl.ds(0, qcols)], load_sem.at[5]),
        pltpu.make_async_copy(gw_hbm, gw, load_sem.at[6]),
        pltpu.make_async_copy(ow_hbm, ow, load_sem.at[7]),
    ]
    for load in loads:
        load.start()

    barrier = pltpu.get_barrier_semaphore()
    pl.semaphore_signal(barrier, inc=1, device_id={"kv": mate}, device_id_type=MESH)
    for d in range(1, tps):
        pl.semaphore_signal(
            barrier, inc=1, device_id={"tp": lax.rem(tp + d, tps)}, device_id_type=MESH
        )

    @pl.when(z > 0)
    def _():
        pl.semaphore_signal(barrier, inc=1, device_id={"kv": me - 2}, device_id_type=MESH)

    ids = chosen_ref[...]

    def make_bias(j, carry):
        for b in range(nq):
            hit = jnp.max(jnp.where(ids == j * nq + b, 0.0, NEGATIVE), axis=1, keepdims=True)
            hit = jnp.broadcast_to(hit, (nq, SEL_BLOCK))
            bias[j, b : b + 1, :] = jnp.concatenate(
                [hit[i : i + 1, :] for i in range(nq)] * group, axis=1
            )
        return carry

    lax.fori_loop(0, me + 1, make_bias, 0)

    def clear(j, carry):
        summ[j] = jnp.zeros((cmp_rows, 2 * kcols), jnp.float32)
        return carry

    lax.fori_loop(me + 1, n, clear, 0)

    for i in range(3):
        loads[i].wait()
    if joint:
        pairs = jnp.dot(
            tok[...], weights[:, qcols : qcols + 2 * kcols], preferred_element_type=jnp.float32
        )
        sides = [pairs[:, :kcols], pairs[:, kcols:]]
    else:
        sides = [
            jnp.dot(tok[...], w[...], preferred_element_type=jnp.float32) for w in (kw, vw)
        ]
    sides = [side.astype(jnp.bfloat16).astype(jnp.float32) for side in sides]
    for i, side in enumerate(sides):
        if not joint:
            side = jnp.concatenate([side, jnp.zeros((rows, 128 - kcols), jnp.float32)], axis=1)
        kvf[i] = side
    keys[me] = sides[0].astype(jnp.bfloat16)
    vals[me] = sides[1].T.astype(jnp.bfloat16)

    def piece(source, part):
        return (keys, vals, summ)[part].at[source]

    def upward(source, part):
        return pltpu.make_async_remote_copy(
            src_ref=piece(source, part),
            dst_ref=piece(source, part),
            send_sem=up_sem.at[source // 2, part],
            recv_sem=recv_sem.at[source, part],
            device_id={"kv": me + 2},
            device_id_type=MESH,
        )

    def across(source, part):
        return pltpu.make_async_remote_copy(
            src_ref=piece(source, part),
            dst_ref=piece(source, part),
            send_sem=across_sem.at[source // 2, part],
            recv_sem=recv_sem.at[source, part],
            device_id={"kv": mate},
            device_id_type=MESH,
        )

    pl.semaphore_wait(barrier, tps + jnp.minimum(chips - 1 - z, 1))

    def send_own(part):
        @pl.when(has_up)
        def _():
            upward(me, part).start()

        @pl.when(core == 0)
        def _():
            across(me, part).start()

    send_own(0)
    send_own(1)

    loads[3].wait()
    loads[4].wait()
    squeezed = []
    for side, weight in ((0, sqk), (1, sqv)):
        tiles = []
        for p in range(0, CMP_LEN, 2):
            a = kvf[side, pl.ds(p, cmp_rows, stride=CMP_LEN), :]
            b = kvf[side, pl.ds(p + 1, cmp_rows, stride=CMP_LEN), :]
            heads = [
                jnp.concatenate([x[:, k * hs : (k + 1) * hs] for x in (a, b)], axis=1)
                for k in range(kvl)
            ]
            tiles.append(jnp.concatenate(heads, axis=0))
        flat = jnp.concatenate(tiles, axis=1).astype(jnp.bfloat16)
        squeezed.append(
            lax.dot_general(flat, weight[...], NT, preferred_element_type=jnp.float32)
            .astype(jnp.bfloat16)
            .astype(jnp.float32)
        )
    summ[me] = jnp.concatenate(
        [
            half[k * cmp_rows : (k + 1) * cmp_rows]
            for half in squeezed
            for k in range(kvl)
        ],
        axis=1,
    )
    send_own(2)

    loads[5].wait()
    scale = hs ** (-0.5)
    queries = (
        jnp.dot(tok[...], weights[:, :qcols], preferred_element_type=jnp.float32)
        .astype(jnp.bfloat16)
        .astype(jnp.float32)
        * scale
    )
    turned = queries.T.astype(jnp.bfloat16)
    for k in range(kvl):
        q[k] = jnp.zeros((kcols, lanes_q), jnp.bfloat16)
        for g in range(group):
            h = k * group + g
            q[k, k * hs : (k + 1) * hs, g * rows : (g + 1) * rows] = turned[
                h * hs : (h + 1) * hs, :
            ]
    loads[6].wait()
    hl = kvl * group
    every = jax.nn.sigmoid(
        lax.dot_general(gw[...], tok[...], NT, preferred_element_type=jnp.float32)
    )
    for branch in range(2):
        base = branch * tps * hl
        mine = every[base : base + hl, :]
        for t in range(1, tps):
            mine = jnp.where(tp == t, every[base + t * hl : base + (t + 1) * hl, :], mine)
        gates[branch, 0:hl, :] = mine

    def weigh(source, first):
        for k in range(kvl):
            s_ref[k] = jnp.dot(keys[source], q[k], preferred_element_type=jnp.float32)
        alphas = []
        for k in range(kvl):
            for tile in range(lanes_q // 128):
                at = pl.ds(tile * 128, 128)
                xs = []
                for b in range(nq):
                    x = s_ref[k, b * SEL_BLOCK : (b + 1) * SEL_BLOCK, at]
                    x = x + bias[source, b : b + 1, at]
                    if first:
                        col = lax.broadcasted_iota(jnp.int32, (SEL_BLOCK, 128), 1)
                        row = lax.broadcasted_iota(jnp.int32, (SEL_BLOCK, 128), 0)
                        seen = row + b * SEL_BLOCK <= col + (tile * 128) % rows
                        x = jnp.where(seen, x, NEGATIVE)
                    xs.append(x.reshape(SEL_BLOCK // 8, 8, 128))
                top = functools.reduce(jnp.maximum, [jnp.max(x, axis=0) for x in xs])
                peak = jnp.max(top, axis=0, keepdims=True)
                if not first:
                    before = m_ref[k, 0:1, at]
                    peak = jnp.maximum(before, peak)
                    alphas.append(jnp.exp(before - peak))
                total = None
                for b in range(nq):
                    p = jnp.exp(xs[b] - peak)
                    part = jnp.sum(p, axis=0)
                    total = part if total is None else total + part
                    p_ref[k, b * SEL_BLOCK : (b + 1) * SEL_BLOCK, at] = p.reshape(
                        SEL_BLOCK, 128
                    ).astype(jnp.bfloat16)
                if not first:
                    total = total + l_ref[k, :, at] * alphas[-1]
                m_ref[k, 0:1, at] = peak
                l_ref[k, :, at] = total
        return alphas

    def gather(source, alphas):
        for k in range(kvl):
            got = jnp.dot(
                vals[source, k * hs : (k + 1) * hs, :],
                p_ref[k],
                preferred_element_type=jnp.float32,
            )
            if alphas:
                tiles = lanes_q // 128
                alpha = jnp.concatenate(alphas[k * tiles : (k + 1) * tiles], axis=1)
                got = got + acc_ref[k] * alpha
            acc_ref[k] = got

    gather(me, weigh(me, True))

    @pl.when(core == 1)
    def _():
        across(me - 1, 0).wait_recv()
        alphas = weigh(me - 1, False)
        across(me - 1, 1).wait_recv()
        gather(me - 1, alphas)
        across(me - 1, 2).wait_recv()

    def step(s, carry):
        mine = me - 2 * s
        other = mate - 2 * s

        def take(part):
            upward(mine, part).wait_recv()

            @pl.when(has_up)
            def _():
                upward(mine, part).start()

            across(mine, part).start()

        take(0)
        alphas = weigh(mine, False)
        take(1)
        gather(mine, alphas)
        across(other, 0).wait_recv()
        alphas = weigh(other, False)
        take(2)
        across(other, 1).wait_recv()
        gather(other, alphas)
        across(other, 2).wait_recv()
        return carry

    lax.fori_loop(1, z + 1, step, 0)

    cols = n * cmp_rows
    small = summ[...].reshape(cols, 2 * kcols)
    small_keys = small[:, :kcols].astype(jnp.bfloat16)
    small_vals = small.T[kcols:, :].astype(jnp.bfloat16)
    col = lax.broadcasted_iota(jnp.int32, (cols, rows), 0)
    row = lax.broadcasted_iota(jnp.int32, (cols, rows), 1)
    seen = col * CMP_LEN + (CMP_LEN - 1) <= row + me * rows
    mixed = []
    for k in range(kvl):
        s = jnp.dot(small_keys, q[k], preferred_element_type=jnp.float32)
        sel = acc_ref[k] / jnp.sum(l_ref[k], axis=0, keepdims=True)
        for g in range(group):
            cut = slice(g * rows, (g + 1) * rows)
            x = jnp.where(seen, s[:, cut], NEGATIVE)
            peak = jnp.max(x, axis=0, keepdims=True)
            w = jnp.where(seen, jnp.exp(x - peak), 0.0)
            total = jnp.maximum(jnp.sum(w, axis=0, keepdims=True), 1.0)
            comp = jnp.dot(
                small_vals[k * hs : (k + 1) * hs, :],
                w.astype(jnp.bfloat16),
                preferred_element_type=jnp.float32,
            )
            h = k * group + g
            mixed.append(
                gates[0, h : h + 1, :] / total * comp + gates[1, h : h + 1, :] * sel[:, cut]
            )
    mix[tp] = jnp.concatenate(mixed, axis=0).T.astype(jnp.bfloat16)

    def swap(ref, d, source, kind):
        return pltpu.make_async_remote_copy(
            src_ref=ref.at[source],
            dst_ref=ref.at[source],
            send_sem=tp_send.at[kind, d],
            recv_sem=tp_recv.at[kind, source],
            device_id={"tp": lax.rem(tp + d, tps)},
            device_id_type=MESH,
        )

    for d in range(1, tps):
        swap(mix, d, tp, 0).start()
    loads[7].wait()
    for d in range(1, tps):
        swap(mix, d, lax.rem(tp + d, tps), 0).wait_recv()
    proj = jnp.dot(mix[0], ow[:qcols, :], preferred_element_type=jnp.float32)
    for t in range(1, tps):
        proj = proj + jnp.dot(
            mix[t], ow[t * qcols : (t + 1) * qcols, :], preferred_element_type=jnp.float32
        )
    lanes = proj[:, :128] * proj[:, :128]
    for i in range(1, proj.shape[1] // 128):
        tile = proj[:, i * 128 : (i + 1) * 128]
        lanes = lanes + tile * tile
    sq[tp] = jnp.sum(lanes.T.reshape(16, 8, rows), axis=0)
    for d in range(1, tps):
        swap(sq, d, tp, 1).start()

    for part in range(parts):
        @pl.when(has_up)
        def _():
            upward(me, part).wait_send()

        @pl.when(core == 0)
        def _():
            across(me, part).wait_send()

    def drain(s, carry):
        mine = me - 2 * s
        for part in range(parts):
            @pl.when(has_up)
            def _():
                upward(mine, part).wait_send()

            across(mine, part).wait_send()
        return carry

    lax.fori_loop(1, z + 1, drain, 0)
    for d in range(1, tps):
        swap(sq, d, lax.rem(tp + d, tps), 1).wait_recv()
    squares = jnp.sum(jnp.sum(sq[...], axis=0), axis=0, keepdims=True)
    factor = lax.rsqrt(squares / total_cols + EPSILON)
    column = jnp.broadcast_to(factor, (128, rows)).T
    width_out = out_ref.shape[1]
    gain = gain_ref[:, :width_out].astype(jnp.float32)
    for t in range(1, tps):
        gain = jnp.where(
            tp == t, gain_ref[:, t * width_out : (t + 1) * width_out].astype(jnp.float32), gain
        )
    for i in range(width_out // 128):
        at = slice(i * 128, (i + 1) * 128)
        out_ref[:, at] = (proj[:, at] * column * gain[:, at]).astype(out_ref.dtype)
    for d in range(1, tps):
        swap(mix, d, tp, 0).wait_send()
        swap(sq, d, tp, 1).wait_send()


def body(
    n,
    tps,
    tokens,
    query_weight,
    key_weight,
    value_weight,
    gate_weight,
    squeeze_key,
    squeeze_value,
    out_weight,
    out_gain,
    chosen,
):
    rows, width = tokens.shape
    hs = squeeze_key.shape[1]
    kvl = key_weight.shape[1] // hs
    qcols = query_weight.shape[1]
    group = qcols // hs // kvl
    cols = out_weight.shape[1]
    total_cols = out_gain.shape[0]
    lanes_q = group * rows
    cmp_rows = rows // CMP_LEN
    dims = (rows, width, hs, kvl, group, total_cols, tps)
    kcols = kvl * hs
    joint = kcols % 128 == 0
    spare = (8, 128) if joint else (width, kcols)
    any_spec = pl.BlockSpec(memory_space=pl.ANY)
    vmem = pl.BlockSpec(memory_space=pltpu.VMEM)
    bf, f32 = jnp.bfloat16, jnp.float32
    dma = pltpu.SemaphoreType.DMA
    return pl.pallas_call(
        functools.partial(kernel, n, dims),
        out_shape=jax.ShapeDtypeStruct((rows, cols), bf),
        in_specs=[vmem] * 2 + [any_spec] * 8,
        out_specs=vmem,
        scratch_shapes=[
            pltpu.VMEM((rows, width), bf),
            pltpu.VMEM((width, qcols + 2 * kcols if joint else qcols), bf),
            pltpu.VMEM(spare, bf),
            pltpu.VMEM(spare, bf),
            pltpu.VMEM((gate_weight.shape[0] * gate_weight.shape[2], width), bf),
            pltpu.VMEM(squeeze_key.shape[::-1], bf),
            pltpu.VMEM(squeeze_value.shape[::-1], bf),
            pltpu.VMEM(out_weight.shape, bf),
            pltpu.VMEM((n, rows, kcols), bf),
            pltpu.VMEM((n, kcols, rows), bf),
            pltpu.VMEM((2, rows, max(kcols, 128)), f32),
            pltpu.VMEM((n, cmp_rows, 2 * kcols), f32),
            pltpu.VMEM((n, 8, lanes_q), f32),
            pltpu.VMEM((kvl, kcols, lanes_q), bf),
            pltpu.VMEM((2, 8, rows), f32),
            pltpu.VMEM((kvl, 8, lanes_q), f32),
            pltpu.VMEM((kvl, 8, lanes_q), f32),
            pltpu.VMEM((kvl, hs, lanes_q), f32),
            pltpu.VMEM((kvl, rows, lanes_q), f32),
            pltpu.VMEM((kvl, rows, lanes_q), bf),
            pltpu.VMEM((tps, rows, qcols), bf),
            pltpu.VMEM((tps, 8, rows), f32),
            dma((8,)),
            dma((n, 3)),
            dma((n // 2, 3)),
            dma((n // 2, 3)),
            dma((2, tps)),
            dma((2, tps)),
        ],
        compiler_params=pltpu.CompilerParams(
            collective_id=0, has_side_effects=True, vmem_limit_bytes=56 * 1024 * 1024
        ),
    )(
        chosen,
        out_gain.reshape(1, -1),
        tokens,
        query_weight,
        key_weight,
        value_weight,
        gate_weight.transpose(0, 2, 1).reshape(-1, width),
        squeeze_key.T,
        squeeze_value.T,
        out_weight,
    )


def solution(mesh):
    in_specs = (
        P(("grp", "kv"), None),
        P(None, "tp"),
        P(None, "tp"),
        P(None, "tp"),
        P(),
        P(),
        P(),
        P(None, "tp"),
        P(),
        P(("grp", "kv"), None),
    )
    return jax.shard_map(
        functools.partial(body, mesh.shape["kv"], mesh.shape["tp"]),
        mesh=mesh,
        in_specs=in_specs,
        out_specs=P(("grp", "kv"), "tp"),
        check_vma=False,
    )
```

time: 32.6 us -> 28.3 us (0.87)
  Pallas kernels: 29.6 us -> 24.9 us
  local copies, waits for them, and re-layouts: 0.69 us -> 3.16 us
  other arithmetic: 2.12 us -> 0 us
    pallas_call x1, Pallas kernels: 29.6 us -> 24.9 us  [body(): pl.pallas_call(functools.partial(kernel, n, dims), out_shape=jax.ShapeDty...]
    convert_element_type x2 -> x0, other arithmetic: 2.12 us -> none  [body(): return (scaled * gain.astype(f32)[None, :]).astype(bf)]
    unnamed x2 -> x3, local copies, waits for them, and re-layouts: 0.69 us -> 2.56 us
    reshape x0 -> x1, local copies, waits for them, and re-layouts: none -> 0.6 us  [body(): out_gain.reshape(1, -1)]
where the time goes in v2:
time: 28.3 us; the launch traced here: 28.1 us
  Pallas kernels  24.9 us (88%)
  local copies, waits for them, and re-layouts  3.16 us (11%)
    pallas_call x1, Pallas kernels, body(): pl.pallas_call(functools.partial(kernel, n, dims), out_shape=jax.ShapeDty...  24.9 us
    unnamed x3, local copies, waits for them, and re-layouts  2.56 us
    reshape x1, local copies, waits for them, and re-layouts, body(): out_gain.reshape(1, -1)  0.6 us

profile of v2, /device:TPU:30, one launch (start us, length us, event | category | flops | bytes accessed | tf_op | source)
XLA Modules:
  0.0 28.1 jit_solution(14197510940365961813)
XLA Ops:
  0.0 0.0 copy-start
  0.0 0.7 %copy-done = bf16[2048]{0:T(1024)(128)(2,1)S(1)} copy-done((bf16[2048]{0:T(1024)(128)(2,1)S(1)}, bf16[2048]{0:T(1024)(128)(2,1)}, u32[]{:S(2)}) %copy-start) | copy-done | bytes 4120
  0.7 0.6 %reshape.6.gain_ref = bf16[1,2048]{1,0:T(2,128)(2,1)} reshape(bf16[2048]{0:T(1024)(128)(2,1)S(1)} %copy-done) | data formatting | bytes 8192 | tf_op jit(solution)/shard_map/reshape | solution.py:489
  1.3 24.9 %shard_map.100 = bf16[256,1024]{1,0:T(8,128)(2,1)} custom-call(s32[4,32]{1,0:T(4,128)} %chosen_ref.1, bf16[1,2048]{1,0:T(2,128)(2,1)} %reshape.6.gain_ref, bf16[256,2048]{1,0:T(8,128)(2,1)} %tok_hbm.1, bf16[2048,256]{1,0:T(8,128)(2,1)} %qw_hbm.1, bf16[2048,128]{1,0:T(8,128)(2,1)} %kw_hbm.1, bf16[2048,128]{1,0:T(8,128)(2,1)} %vw_hbm.1, ...), custom_call_target="tpu_custom_call" | custom-call | tf_op jit(solution)/shard_map/pallas_call | solution.py:449
  26.2 1.9 %copy.12 = bf16[256,1024]{1,0:T(8,128)(2,1)} copy(bf16[256,1024]{1,0:T(8,128)(2,1)} %shard_map.100) | data formatting | bytes 1048576
Async XLA Ops:
  0.0 0.7 %copy-start = (bf16[2048]{0:T(1024)(128)(2,1)S(1)}, bf16[2048]{0:T(1024)(128)(2,1)}, u32[]{:S(2)}) copy-start(bf16[2048]{0:T(1024)(128)(2,1)} %param.18) | copy-start | bytes 12292

commit v3 on v2

--- a/solution.py
+++ b/solution.py
@@ -19,7 +19,6 @@
     n,
     dims,
     chosen_ref,
-    gain_ref,
     tok_hbm,
     qw_hbm,
     kw_hbm,
@@ -28,6 +27,7 @@
     sqk_hbm,
     sqv_hbm,
     ow_hbm,
+    gain_hbm,
     out_ref,
     tok,
     weights,
@@ -37,6 +37,7 @@
     sqk,
     sqv,
     ow,
+    gain_ref,
     keys,
     vals,
     kvf,
@@ -49,6 +50,7 @@
     acc_ref,
     s_ref,
     p_ref,
+    comp_ref,
     mix,
     sq,
     load_sem,
@@ -77,18 +79,29 @@
     if joint:
         kw = weights.at[:, pl.ds(qcols, kcols)]
         vw = weights.at[:, pl.ds(qcols + kcols, kcols)]
-    loads = [
-        pltpu.make_async_copy(tok_hbm, tok, load_sem.at[0]),
-        pltpu.make_async_copy(kw_hbm, kw, load_sem.at[1]),
-        pltpu.make_async_copy(vw_hbm, vw, load_sem.at[2]),
-        pltpu.make_async_copy(sqk_hbm, sqk, load_sem.at[3]),
-        pltpu.make_async_copy(sqv_hbm, sqv, load_sem.at[4]),
-        pltpu.make_async_copy(qw_hbm, weights.at[:, pl.ds(0, qcols)], load_sem.at[5]),
-        pltpu.make_async_copy(gw_hbm, gw, load_sem.at[6]),
-        pltpu.make_async_copy(ow_hbm, ow, load_sem.at[7]),
-    ]
-    for load in loads:
-        load.start()
+    chunks = load_sem.shape[0] // 3 - 2
+    step_w = width // chunks
+    spots = [pl.ds(c * step_w, step_w) for c in range(chunks)]
+    first_loads = []
+    for c, spot in enumerate(spots):
+        first_loads.append(
+            [
+                pltpu.make_async_copy(
+                    tok_hbm.at[:, spot], tok.at[:, spot], load_sem.at[6 + 3 * c]
+                ),
+                pltpu.make_async_copy(kw_hbm.at[spot], kw.at[spot], load_sem.at[7 + 3 * c]),
+                pltpu.make_async_copy(vw_hbm.at[spot], vw.at[spot], load_sem.at[8 + 3 * c]),
+            ]
+        )
+    for group_loads in first_loads:
+        for load in group_loads:
+            load.start()
+    load_sqk = pltpu.make_async_copy(sqk_hbm, sqk, load_sem.at[0])
+    load_sqv = pltpu.make_async_copy(sqv_hbm, sqv, load_sem.at[1])
+    load_qw = pltpu.make_async_copy(qw_hbm, weights.at[:, pl.ds(0, qcols)], load_sem.at[2])
+    load_gw = pltpu.make_async_copy(gw_hbm, gw, load_sem.at[3])
+    load_ow = pltpu.make_async_copy(ow_hbm, ow, load_sem.at[4])
+    load_gain = pltpu.make_async_copy(gain_hbm, gain_ref, load_sem.at[5])
 
     barrier = pltpu.get_barrier_semaphore()
     pl.semaphore_signal(barrier, inc=1, device_id={"kv": mate}, device_id_type=MESH)
@@ -120,17 +133,28 @@
 
     lax.fori_loop(me + 1, n, clear, 0)
 
-    for i in range(3):
-        loads[i].wait()
-    if joint:
-        pairs = jnp.dot(
-            tok[...], weights[:, qcols : qcols + 2 * kcols], preferred_element_type=jnp.float32
-        )
-        sides = [pairs[:, :kcols], pairs[:, kcols:]]
-    else:
-        sides = [
-            jnp.dot(tok[...], w[...], preferred_element_type=jnp.float32) for w in (kw, vw)
-        ]
+    totals = [None, None]
+    for c, spot in enumerate(spots):
+        for load in first_loads[c]:
+            load.wait()
+        if c == chunks - 1:
+            for load in (load_sqk, load_sqv, load_qw, load_gw, load_ow, load_gain):
+                load.start()
+        piece_tok = tok[:, spot]
+        if joint:
+            got = jnp.dot(
+                piece_tok,
+                weights[spot, qcols : qcols + 2 * kcols],
+                preferred_element_type=jnp.float32,
+            )
+            got = [got[:, :kcols], got[:, kcols:]]
+        else:
+            got = [
+                jnp.dot(piece_tok, w[spot, :], preferred_element_type=jnp.float32)
+                for w in (kw, vw)
+            ]
+        totals = [g if t is None else t + g for t, g in zip(totals, got)]
+    sides = totals
     sides = [side.astype(jnp.bfloat16).astype(jnp.float32) for side in sides]
     for i, side in enumerate(sides):
         if not joint:
@@ -140,7 +164,7 @@
     vals[me] = sides[1].T.astype(jnp.bfloat16)
 
     def piece(source, part):
-        return (keys, vals, summ)[part].at[source]
+        return (keys, summ, vals)[part].at[source]
 
     def upward(source, part):
         return pltpu.make_async_remote_copy(
@@ -174,10 +198,9 @@
             across(me, part).start()
 
     send_own(0)
-    send_own(1)
-
-    loads[3].wait()
-    loads[4].wait()
+
+    load_sqk.wait()
+    load_sqv.wait()
     squeezed = []
     for side, weight in ((0, sqk), (1, sqv)):
         tiles = []
@@ -203,9 +226,10 @@
         ],
         axis=1,
     )
+    send_own(1)
     send_own(2)
 
-    loads[5].wait()
+    load_qw.wait()
     scale = hs ** (-0.5)
     queries = (
         jnp.dot(tok[...], weights[:, :qcols], preferred_element_type=jnp.float32)
@@ -221,7 +245,7 @@
             q[k, k * hs : (k + 1) * hs, g * rows : (g + 1) * rows] = turned[
                 h * hs : (h + 1) * hs, :
             ]
-    loads[6].wait()
+    load_gw.wait()
     hl = kvl * group
     every = jax.nn.sigmoid(
         lax.dot_general(gw[...], tok[...], NT, preferred_element_type=jnp.float32)
@@ -233,7 +257,7 @@
             mine = jnp.where(tp == t, every[base + t * hl : base + (t + 1) * hl, :], mine)
         gates[branch, 0:hl, :] = mine
 
-    def weigh(source, first):
+    def weigh(source, first, slot=0):
         for k in range(kvl):
             s_ref[k] = jnp.dot(keys[source], q[k], preferred_element_type=jnp.float32)
         alphas = []
@@ -261,7 +285,7 @@
                     p = jnp.exp(xs[b] - peak)
                     part = jnp.sum(p, axis=0)
                     total = part if total is None else total + part
-                    p_ref[k, b * SEL_BLOCK : (b + 1) * SEL_BLOCK, at] = p.reshape(
+                    p_ref[slot, k, b * SEL_BLOCK : (b + 1) * SEL_BLOCK, at] = p.reshape(
                         SEL_BLOCK, 128
                     ).astype(jnp.bfloat16)
                 if not first:
@@ -270,11 +294,11 @@
                 l_ref[k, :, at] = total
         return alphas
 
-    def gather(source, alphas):
+    def gather(source, alphas, slot=0):
         for k in range(kvl):
             got = jnp.dot(
                 vals[source, k * hs : (k + 1) * hs, :],
-                p_ref[k],
+                p_ref[slot, k],
                 preferred_element_type=jnp.float32,
             )
             if alphas:
@@ -285,13 +309,43 @@
 
     gather(me, weigh(me, True))
 
+    cols = n * cmp_rows
+
+    def compress():
+        small = summ[...].reshape(cols, 2 * kcols)
+        small_keys = small[:, :kcols].astype(jnp.bfloat16)
+        small_vals = small.T[kcols:, :].astype(jnp.bfloat16)
+        col = lax.broadcasted_iota(jnp.int32, (cols, rows), 0)
+        row = lax.broadcasted_iota(jnp.int32, (cols, rows), 1)
+        seen = col * CMP_LEN + (CMP_LEN - 1) <= row + me * rows
+        for k in range(kvl):
+            s = jnp.dot(small_keys, q[k], preferred_element_type=jnp.float32)
+            for g in range(group):
+                x = jnp.where(seen, s[:, g * rows : (g + 1) * rows], NEGATIVE)
+                peak = jnp.max(x, axis=0, keepdims=True)
+                w = jnp.where(seen, jnp.exp(x - peak), 0.0)
+                total = jnp.maximum(jnp.sum(w, axis=0, keepdims=True), 1.0)
+                comp = jnp.dot(
+                    small_vals[k * hs : (k + 1) * hs, :],
+                    w.astype(jnp.bfloat16),
+                    preferred_element_type=jnp.float32,
+                )
+                h = k * group + g
+                comp_ref[k, :, g * rows : (g + 1) * rows] = comp * (
+                    gates[0, h : h + 1, :] / total
+                )
+
     @pl.when(core == 1)
     def _():
         across(me - 1, 0).wait_recv()
         alphas = weigh(me - 1, False)
         across(me - 1, 1).wait_recv()
+        across(me - 1, 2).wait_recv()
         gather(me - 1, alphas)
-        across(me - 1, 2).wait_recv()
+
+    @pl.when(z == 0)
+    def _():
+        compress()
 
     def step(s, carry):
         mine = me - 2 * s
@@ -309,72 +363,65 @@
         take(0)
         alphas = weigh(mine, False)
         take(1)
+        across(other, 0).wait_recv()
+        alphas_other = weigh(other, False, 1)
+        across(other, 1).wait_recv()
+
+        @pl.when(s == z)
+        def _():
+            compress()
+
+        take(2)
         gather(mine, alphas)
-        across(other, 0).wait_recv()
-        alphas = weigh(other, False)
-        take(2)
-        across(other, 1).wait_recv()
-        gather(other, alphas)
         across(other, 2).wait_recv()
+        gather(other, alphas_other, 1)
         return carry
 
     lax.fori_loop(1, z + 1, step, 0)
-
-    cols = n * cmp_rows
-    small = summ[...].reshape(cols, 2 * kcols)
-    small_keys = small[:, :kcols].astype(jnp.bfloat16)
-    small_vals = small.T[kcols:, :].astype(jnp.bfloat16)
-    col = lax.broadcasted_iota(jnp.int32, (cols, rows), 0)
-    row = lax.broadcasted_iota(jnp.int32, (cols, rows), 1)
-    seen = col * CMP_LEN + (CMP_LEN - 1) <= row + me * rows
-    mixed = []
-    for k in range(kvl):
-        s = jnp.dot(small_keys, q[k], preferred_element_type=jnp.float32)
-        sel = acc_ref[k] / jnp.sum(l_ref[k], axis=0, keepdims=True)
-        for g in range(group):
-            cut = slice(g * rows, (g + 1) * rows)
-            x = jnp.where(seen, s[:, cut], NEGATIVE)
-            peak = jnp.max(x, axis=0, keepdims=True)
-            w = jnp.where(seen, jnp.exp(x - peak), 0.0)
-            total = jnp.maximum(jnp.sum(w, axis=0, keepdims=True), 1.0)
-            comp = jnp.dot(
-                small_vals[k * hs : (k + 1) * hs, :],
-                w.astype(jnp.bfloat16),
-                preferred_element_type=jnp.float32,
-            )
-            h = k * group + g
-            mixed.append(
-                gates[0, h : h + 1, :] / total * comp + gates[1, h : h + 1, :] * sel[:, cut]
-            )
-    mix[tp] = jnp.concatenate(mixed, axis=0).T.astype(jnp.bfloat16)
 
     def swap(ref, d, source, kind):
         return pltpu.make_async_remote_copy(
             src_ref=ref.at[source],
             dst_ref=ref.at[source],
             send_sem=tp_send.at[kind, d],
-            recv_sem=tp_recv.at[kind, source],
+            recv_sem=tp_recv.at[kind, source // (kvl if kind < kvl else 1)],
             device_id={"tp": lax.rem(tp + d, tps)},
             device_id_type=MESH,
         )
 
-    for d in range(1, tps):
-        swap(mix, d, tp, 0).start()
-    loads[7].wait()
-    for d in range(1, tps):
-        swap(mix, d, lax.rem(tp + d, tps), 0).wait_recv()
-    proj = jnp.dot(mix[0], ow[:qcols, :], preferred_element_type=jnp.float32)
-    for t in range(1, tps):
-        proj = proj + jnp.dot(
-            mix[t], ow[t * qcols : (t + 1) * qcols, :], preferred_element_type=jnp.float32
-        )
+    for k in range(kvl):
+        sel = acc_ref[k] / jnp.sum(l_ref[k], axis=0, keepdims=True)
+        mixed = []
+        for g in range(group):
+            h = k * group + g
+            at = slice(g * rows, (g + 1) * rows)
+            mixed.append(comp_ref[k, :, at] + gates[1, h : h + 1, :] * sel[:, at])
+        mix[tp * kvl + k] = jnp.concatenate(mixed, axis=0).T.astype(jnp.bfloat16)
+        for d in range(1, tps):
+            swap(mix, d, tp * kvl + k, k).start()
+    load_ow.wait()
+    load_gain.wait()
+    tall = group * hs
+
+    def product(t, k):
+        at = pl.ds(pl.multiple_of((t * kvl + k) * tall, tall), tall)
+        return jnp.dot(mix[t * kvl + k], ow[at, :], preferred_element_type=jnp.float32)
+
+    proj = product(tp, 0)
+    for k in range(1, kvl):
+        proj = proj + product(tp, k)
+    for k in range(kvl):
+        for d in range(1, tps):
+            t = lax.rem(tp + d, tps)
+            swap(mix, d, t * kvl + k, k).wait_recv()
+            proj = proj + product(t, k)
     lanes = proj[:, :128] * proj[:, :128]
     for i in range(1, proj.shape[1] // 128):
         tile = proj[:, i * 128 : (i + 1) * 128]
         lanes = lanes + tile * tile
     sq[tp] = jnp.sum(lanes.T.reshape(16, 8, rows), axis=0)
     for d in range(1, tps):
-        swap(sq, d, tp, 1).start()
+        swap(sq, d, tp, kvl).start()
 
     for part in range(parts):
         @pl.when(has_up)
@@ -397,22 +444,22 @@
 
     lax.fori_loop(1, z + 1, drain, 0)
     for d in range(1, tps):
-        swap(sq, d, lax.rem(tp + d, tps), 1).wait_recv()
+        swap(sq, d, lax.rem(tp + d, tps), kvl).wait_recv()
     squares = jnp.sum(jnp.sum(sq[...], axis=0), axis=0, keepdims=True)
     factor = lax.rsqrt(squares / total_cols + EPSILON)
     column = jnp.broadcast_to(factor, (128, rows)).T
     width_out = out_ref.shape[1]
-    gain = gain_ref[:, :width_out].astype(jnp.float32)
+    gain_all = gain_ref[...].astype(jnp.float32).reshape(1, total_cols)
+    gain = gain_all[:, :width_out]
     for t in range(1, tps):
-        gain = jnp.where(
-            tp == t, gain_ref[:, t * width_out : (t + 1) * width_out].astype(jnp.float32), gain
-        )
+        gain = jnp.where(tp == t, gain_all[:, t * width_out : (t + 1) * width_out], gain)
     for i in range(width_out // 128):
         at = slice(i * 128, (i + 1) * 128)
         out_ref[:, at] = (proj[:, at] * column * gain[:, at]).astype(out_ref.dtype)
     for d in range(1, tps):
-        swap(mix, d, tp, 0).wait_send()
-        swap(sq, d, tp, 1).wait_send()
+        for k in range(kvl):
+            swap(mix, d, tp * kvl + k, k).wait_send()
+        swap(sq, d, tp, kvl).wait_send()
 
 
 def body(
@@ -442,14 +489,14 @@
     kcols = kvl * hs
     joint = kcols % 128 == 0
     spare = (8, 128) if joint else (width, kcols)
-    any_spec = pl.BlockSpec(memory_space=pl.ANY)
+    any_spec = pl.BlockSpec(memory_space=pltpu.HBM)
     vmem = pl.BlockSpec(memory_space=pltpu.VMEM)
     bf, f32 = jnp.bfloat16, jnp.float32
     dma = pltpu.SemaphoreType.DMA
     return pl.pallas_call(
         functools.partial(kernel, n, dims),
         out_shape=jax.ShapeDtypeStruct((rows, cols), bf),
-        in_specs=[vmem] * 2 + [any_spec] * 8,
+        in_specs=[vmem] + [any_spec] * 9,
         out_specs=vmem,
         scratch_shapes=[
             pltpu.VMEM((rows, width), bf),
@@ -460,6 +507,7 @@
             pltpu.VMEM(squeeze_key.shape[::-1], bf),
             pltpu.VMEM(squeeze_value.shape[::-1], bf),
             pltpu.VMEM(out_weight.shape, bf),
+            pltpu.VMEM(out_gain.shape, bf),
             pltpu.VMEM((n, rows, kcols), bf),
             pltpu.VMEM((n, kcols, rows), bf),
             pltpu.VMEM((2, rows, max(kcols, 128)), f32),
@@ -471,22 +519,22 @@
             pltpu.VMEM((kvl, 8, lanes_q), f32),
             pltpu.VMEM((kvl, hs, lanes_q), f32),
             pltpu.VMEM((kvl, rows, lanes_q), f32),
-            pltpu.VMEM((kvl, rows, lanes_q), bf),
-            pltpu.VMEM((tps, rows, qcols), bf),
+            pltpu.VMEM((2, kvl, rows, lanes_q), bf),
+            pltpu.VMEM((kvl, hs, lanes_q), f32),
+            pltpu.VMEM((tps * kvl, rows, group * hs), bf),
             pltpu.VMEM((tps, 8, rows), f32),
-            dma((8,)),
+            dma((18,)),
             dma((n, 3)),
             dma((n // 2, 3)),
             dma((n // 2, 3)),
-            dma((2, tps)),
-            dma((2, tps)),
+            dma((kvl + 1, tps)),
+            dma((kvl + 1, tps)),
         ],
         compiler_params=pltpu.CompilerParams(
-            collective_id=0, has_side_effects=True, vmem_limit_bytes=56 * 1024 * 1024
+            collective_id=0, has_side_effects=True, vmem_limit_bytes=28 * 1024 * 1024
         ),
     )(
         chosen,
-        out_gain.reshape(1, -1),
         tokens,
         query_weight,
         key_weight,
@@ -495,6 +543,7 @@
         squeeze_key.T,
         squeeze_value.T,
         out_weight,
+        out_gain,
     )
 
 

time: 28.3 us -> 34.1 us (1.20)
  local copies, waits for them, and re-layouts: 3.16 us -> 10.7 us
  Pallas kernels: 24.9 us -> 23 us
    unnamed x3 -> x21, local copies, waits for them, and re-layouts: 2.56 us -> 10.7 us
    pallas_call x1, Pallas kernels: 24.9 us -> 23 us  [body(): pl.pallas_call(functools.partial(kernel, n, dims), out_shape=jax.ShapeDty...]
    reshape x1 -> x0, local copies, waits for them, and re-layouts: 0.6 us -> none  [body(): out_gain.reshape(1, -1)]
where the time goes in v3:
time: 34.1 us; the launch traced here: 33.6 us
  Pallas kernels  23 us (67%)
  local copies, waits for them, and re-layouts  10.7 us (31%)
    pallas_call x1, Pallas kernels, body(): pl.pallas_call(functools.partial(kernel, n, dims), out_shape=jax.ShapeDty...  23 us
    unnamed x21, local copies, waits for them, and re-layouts  10.7 us

profile of v3, /device:TPU:30, one launch (start us, length us, event | category | flops | bytes accessed | tf_op | source)
XLA Modules:
  0.0 33.6 jit_solution(10497031596538154032)
XLA Ops:
  0.0 0.0 copy-start.8
  0.0 0.7 %copy-done.8 = bf16[2048]{0:T(1024)(128)(2,1)S(1)} copy-done((bf16[2048]{0:T(1024)(128)(2,1)S(1)}, bf16[2048]{0:T(1024)(128)(2,1)}, u32[]{:S(2)}) %copy-start.8) | copy-done | bytes 4120
  0.7 0.0 copy-start
  0.7 1.2 %copy-done = bf16[256,2048]{1,0:T(8,128)(2,1)S(1)} copy-done((bf16[256,2048]{1,0:T(8,128)(2,1)S(1)}, bf16[256,2048]{1,0:T(8,128)(2,1)}, u32[]{:S(2)}) %copy-start) | copy-done | bytes 1048600
  1.9 0.0 copy-start.1
  1.9 1.2 %copy-done.1 = bf16[2048,256]{1,0:T(8,128)(2,1)S(1)} copy-done((bf16[2048,256]{1,0:T(8,128)(2,1)S(1)}, bf16[2048,256]{1,0:T(8,128)(2,1)}, u32[]{:S(2)}) %copy-start.1) | copy-done | bytes 1048600
  3.1 0.0 copy-start.2
  3.1 1.2 %copy-done.2 = bf16[512,1024]{1,0:T(8,128)(2,1)S(1)} copy-done((bf16[512,1024]{1,0:T(8,128)(2,1)S(1)}, bf16[512,1024]{1,0:T(8,128)(2,1)}, u32[]{:S(2)}) %copy-start.2) | copy-done | bytes 1048600
  4.4 0.0 copy-start.3
  4.4 1.0 %copy-done.3 = bf16[2048,128]{1,0:T(8,128)(2,1)S(1)} copy-done((bf16[2048,128]{1,0:T(8,128)(2,1)S(1)}, bf16[2048,128]{1,0:T(8,128)(2,1)}, u32[]{:S(2)}) %copy-start.3) | copy-done | bytes 524312
  5.4 0.0 copy-start.4
  5.4 1.0 %copy-done.4 = bf16[2048,128]{1,0:T(8,128)(2,1)S(1)} copy-done((bf16[2048,128]{1,0:T(8,128)(2,1)S(1)}, bf16[2048,128]{1,0:T(8,128)(2,1)}, u32[]{:S(2)}) %copy-start.4) | copy-done | bytes 524312
  6.4 0.0 copy-start.5
  6.5 0.9 %copy-done.5 = bf16[2048,64]{0,1:T(8,128)(2,1)S(1)} copy-done((bf16[2048,64]{0,1:T(8,128)(2,1)S(1)}, bf16[2048,64]{0,1:T(8,128)(2,1)}, u32[]{:S(2)}) %copy-start.5) | copy-done | bytes 262168
  7.4 0.0 copy-start.6
  7.4 0.9 %copy-done.6 = bf16[2048,64]{0,1:T(8,128)(2,1)S(1)} copy-done((bf16[2048,64]{0,1:T(8,128)(2,1)S(1)}, bf16[2048,64]{0,1:T(8,128)(2,1)}, u32[]{:S(2)}) %copy-start.6) | copy-done | bytes 262168
  8.3 0.0 copy-start.7
  8.4 0.8 %copy-done.7 = bf16[2,2048,8]{1,2,0:T(8,128)(2,1)S(1)} copy-done((bf16[2,2048,8]{1,2,0:T(8,128)(2,1)S(1)}, bf16[2,2048,8]{1,2,0:T(8,128)(2,1)}, u32[]{:S(2)}) %copy-start.7) | copy-done | bytes 65560
  9.2 0.0 copy-start.9
  9.2 0.7 %copy-done.9 = s32[4,32]{1,0:T(4,128)S(1)} copy-done((s32[4,32]{1,0:T(4,128)S(1)}, s32[4,32]{1,0:T(4,128)}, u32[]{:S(2)}) %copy-start.9) | copy-done | bytes 536
  9.9 23.0 %shard_map.100 = bf16[256,1024]{1,0:T(8,128)(2,1)S(1)} custom-call(s32[4,32]{1,0:T(4,128)S(1)} %copy-done.9, bf16[256,2048]{1,0:T(8,128)(2,1)S(1)} %copy-done, bf16[2048,256]{1,0:T(8,128)(2,1)S(1)} %copy-done.1, bf16[2048,128]{1,0:T(8,128)(2,1)S(1)} %copy-done.3, bf16[2048,128]{1,0:T(8,128)(2,1)S(1)} %copy-done.4, bf16[16,2048]{1,0:T(8,128)(2,1)S(1)} %bitcast.7, ...), custom_call_target="tpu_custom_call" | custom-call | tf_op jit(solution)/shard_map/pallas_call | solution.py:496
  32.8 0.8 %copy.12 = bf16[256,1024]{1,0:T(8,128)(2,1)} copy(bf16[256,1024]{1,0:T(8,128)(2,1)S(1)} %shard_map.100) | data formatting | bytes 1048576
Async XLA Ops:
  0.0 0.7 %copy-start.8 = (bf16[2048]{0:T(1024)(128)(2,1)S(1)}, bf16[2048]{0:T(1024)(128)(2,1)}, u32[]{:S(2)}) copy-start(bf16[2048]{0:T(1024)(128)(2,1)} %gain_hbm.1) | copy-start | bytes 12292
  0.7 1.2 %copy-start = (bf16[256,2048]{1,0:T(8,128)(2,1)S(1)}, bf16[256,2048]{1,0:T(8,128)(2,1)}, u32[]{:S(2)}) copy-start(bf16[256,2048]{1,0:T(8,128)(2,1)} %tok_hbm.1) | copy-start | bytes 3145732
  1.9 1.2 %copy-start.1 = (bf16[2048,256]{1,0:T(8,128)(2,1)S(1)}, bf16[2048,256]{1,0:T(8,128)(2,1)}, u32[]{:S(2)}) copy-start(bf16[2048,256]{1,0:T(8,128)(2,1)} %qw_hbm.1) | copy-start | bytes 3145732
  3.1 1.2 %copy-start.2 = (bf16[512,1024]{1,0:T(8,128)(2,1)S(1)}, bf16[512,1024]{1,0:T(8,128)(2,1)}, u32[]{:S(2)}) copy-start(bf16[512,1024]{1,0:T(8,128)(2,1)} %ow_hbm.1) | copy-start | bytes 3145732
  4.4 1.0 %copy-start.3 = (bf16[2048,128]{1,0:T(8,128)(2,1)S(1)}, bf16[2048,128]{1,0:T(8,128)(2,1)}, u32[]{:S(2)}) copy-start(bf16[2048,128]{1,0:T(8,128)(2,1)} %kw_hbm.1) | copy-start | bytes 1572868
  5.4 1.0 %copy-start.4 = (bf16[2048,128]{1,0:T(8,128)(2,1)S(1)}, bf16[2048,128]{1,0:T(8,128)(2,1)}, u32[]{:S(2)}) copy-start(bf16[2048,128]{1,0:T(8,128)(2,1)} %vw_hbm.1) | copy-start | bytes 1572868
  6.4 0.9 %copy-start.5 = (bf16[2048,64]{0,1:T(8,128)(2,1)S(1)}, bf16[2048,64]{0,1:T(8,128)(2,1)}, u32[]{:S(2)}) copy-start(bf16[2048,64]{0,1:T(8,128)(2,1)} %param.15) | copy-start | bytes 786436
  7.4 0.9 %copy-start.6 = (bf16[2048,64]{0,1:T(8,128)(2,1)S(1)}, bf16[2048,64]{0,1:T(8,128)(2,1)}, u32[]{:S(2)}) copy-start(bf16[2048,64]{0,1:T(8,128)(2,1)} %param.16) | copy-start | bytes 786436
  8.3 0.8 %copy-start.7 = (bf16[2,2048,8]{1,2,0:T(8,128)(2,1)S(1)}, bf16[2,2048,8]{1,2,0:T(8,128)(2,1)}, u32[]{:S(2)}) copy-start(bf16[2,2048,8]{1,2,0:T(8,128)(2,1)} %param.14) | copy-start | bytes 196612
  9.2 0.7 %copy-start.9 = (s32[4,32]{1,0:T(4,128)S(1)}, s32[4,32]{1,0:T(4,128)}, u32[]{:S(2)}) copy-start(s32[4,32]{1,0:T(4,128)} %chosen_ref.1) | copy-start | bytes 1540

commit v4 on v3

--- a/solution.py
+++ b/solution.py
@@ -489,7 +489,7 @@
     kcols = kvl * hs
     joint = kcols % 128 == 0
     spare = (8, 128) if joint else (width, kcols)
-    any_spec = pl.BlockSpec(memory_space=pltpu.HBM)
+    any_spec = pl.BlockSpec(memory_space=pl.ANY)
     vmem = pl.BlockSpec(memory_space=pltpu.VMEM)
     bf, f32 = jnp.bfloat16, jnp.float32
     dma = pltpu.SemaphoreType.DMA
@@ -531,7 +531,7 @@
             dma((kvl + 1, tps)),
         ],
         compiler_params=pltpu.CompilerParams(
-            collective_id=0, has_side_effects=True, vmem_limit_bytes=28 * 1024 * 1024
+            collective_id=0, has_side_effects=True, vmem_limit_bytes=56 * 1024 * 1024
         ),
     )(
         chosen,

time: 34.1 us -> 26.8 us (0.79)
  local copies, waits for them, and re-layouts: 10.7 us -> 1.87 us
  Pallas kernels: 23 us -> 24.8 us
    unnamed x21 -> x1, local copies, waits for them, and re-layouts: 10.7 us -> 1.87 us
    pallas_call x1, Pallas kernels: 23 us -> 24.8 us  [body(): pl.pallas_call(functools.partial(kernel, n, dims), out_shape=jax.ShapeDty...]
where the time goes in v4:
time: 26.8 us; the launch traced here: 26.6 us
  Pallas kernels  24.8 us (93%)
  local copies, waits for them, and re-layouts  1.87 us (7%)
    pallas_call x1, Pallas kernels, body(): pl.pallas_call(functools.partial(kernel, n, dims), out_shape=jax.ShapeDty...  24.8 us
    unnamed x1, local copies, waits for them, and re-layouts  1.87 us

profile of v4, /device:TPU:30, one launch (start us, length us, event | category | flops | bytes accessed | tf_op | source)
XLA Modules:
  0.0 26.6 jit_solution(9448334842461168952)
XLA Ops:
  0.0 24.8 %shard_map.100 = bf16[256,1024]{1,0:T(8,128)(2,1)} custom-call(s32[4,32]{1,0:T(4,128)} %chosen_ref.1, bf16[256,2048]{1,0:T(8,128)(2,1)} %tok_hbm.1, bf16[2048,256]{1,0:T(8,128)(2,1)} %qw_hbm.1, bf16[2048,128]{1,0:T(8,128)(2,1)} %kw_hbm.1, bf16[2048,128]{1,0:T(8,128)(2,1)} %vw_hbm.1, bf16[16,2048]{1,0:T(8,128)(2,1)} %bitcast.7, bf16[64,2048]{1,0:T(8,128)(2,1)} %bitcast.5, ...), custom_call_target="tpu_custom_call" | custom-call | tf_op jit(solution)/shard_map/pallas_call | solution.py:496
  24.8 1.9 %copy.12 = bf16[256,1024]{1,0:T(8,128)(2,1)} copy(bf16[256,1024]{1,0:T(8,128)(2,1)} %shard_map.100) | data formatting | bytes 1048576

commit v5 on v4

--- a/solution.py
+++ b/solution.py
@@ -137,7 +137,7 @@
     for c, spot in enumerate(spots):
         for load in first_loads[c]:
             load.wait()
-        if c == chunks - 1:
+        if c == 0:
             for load in (load_sqk, load_sqv, load_qw, load_gw, load_ow, load_gain):
                 load.start()
         piece_tok = tok[:, spot]

time: 26.8 us -> 26.7 us (level)
  no operation moved by 1% of the time
where the time goes in v5:
time: 26.7 us; the launch traced here: 26.5 us
  Pallas kernels  24.6 us (92%)
  local copies, waits for them, and re-layouts  1.87 us (7%)
    pallas_call x1, Pallas kernels, body(): pl.pallas_call(functools.partial(kernel, n, dims), out_shape=jax.ShapeDty...  24.6 us
    unnamed x1, local copies, waits for them, and re-layouts  1.87 us

profile of v5, /device:TPU:30, one launch (start us, length us, event | category | flops | bytes accessed | tf_op | source)
XLA Modules:
  0.0 26.5 jit_solution(14178960500952022710)
XLA Ops:
  0.0 24.6 %shard_map.100 = bf16[256,1024]{1,0:T(8,128)(2,1)} custom-call(s32[4,32]{1,0:T(4,128)} %chosen_ref.1, bf16[256,2048]{1,0:T(8,128)(2,1)} %tok_hbm.1, bf16[2048,256]{1,0:T(8,128)(2,1)} %qw_hbm.1, bf16[2048,128]{1,0:T(8,128)(2,1)} %kw_hbm.1, bf16[2048,128]{1,0:T(8,128)(2,1)} %vw_hbm.1, bf16[16,2048]{1,0:T(8,128)(2,1)} %bitcast.7, bf16[64,2048]{1,0:T(8,128)(2,1)} %bitcast.5, ...), custom_call_target="tpu_custom_call" | custom-call | tf_op jit(solution)/shard_map/pallas_call | solution.py:496
  24.6 1.9 %copy.12 = bf16[256,1024]{1,0:T(8,128)(2,1)} copy(bf16[256,1024]{1,0:T(8,128)(2,1)} %shard_map.100) | data formatting | bytes 1048576
